TPU v7x, 32 devices: a whole 2x2x4 slice. The times are simulated.
32 devices in a mesh: sp: 8 (over z, y), tp: 4 (over x, core).
Axes of the slice: x: 2, y: 2, z: 4, core: 2. Of those that a mesh axis runs over, the one named last changes fastest.
Arguments:
- resid: bfloat16 [12288, 2048], P(('sp', 'tp')), may hold values from -6 to 6
- cond: bfloat16 [2048], P('sp'), may hold values from -6 to 6
- mod_shift: bfloat16 [2048, 2048], P('sp', 'tp'), may hold values from -0.125 to 0.125
- mod_scale: bfloat16 [2048, 2048], P('sp', 'tp'), may hold values from -0.125 to 0.125
- mod_gate: bfloat16 [2048, 2048], P('sp', 'tp'), may hold values from -0.125 to 0.125
- norm_gain: float32 [2048], replicated, may hold values from 0.1 to 1.9
- context: bfloat16 [512, 2048], P('sp'), may hold values from -6 to 6
- w_query: bfloat16 [2048, 2048], P(None, 'tp'), may hold values from -0.125 to 0.125
- w_key: bfloat16 [2048, 2048], P(None, 'tp'), may hold values from -0.125 to 0.125
- w_value: bfloat16 [2048, 2048], P(None, 'tp'), may hold values from -0.125 to 0.125
- query_gain: float32 [128], replicated, may hold values from 0.5 to 6, as said below
- key_gain: float32 [128], replicated, may hold values from 0.5 to 6, as said below
- offset_bias: float32 [16, 15, 31], P('tp'), may hold values from -4 to 4
- context_bias: float32 [16], P('tp'), may hold values from -4.5 to 1
- w_out: bfloat16 [2048, 2048], replicated, may hold values from -0.5 to 0.5
Outputs:
- mixed: bfloat16 [12288, 2048], P(('sp', 'tp'))
Inputs may be any that keep to these rules, and one draw needn't show every extreme that they name: `query_gain`: positive gains. `key_gain`: positive gains.
All inputs are finite; a program needn't handle non-finite values.
Results may differ from a plain program's by a relative error of at most 0.0085.
The roundings to bfloat16 on the way count: a program that leaves them out, or rounds other values in their place, can miss the bound.
Values may be sent and summed in bfloat16 or wider, within the bound.
A program may use at most 128 MiB of HBM per device.

v0:
```python
import functools

import jax
import jax.numpy as jnp
from jax import lax
from jax.experimental import pallas as pl
from jax.experimental.pallas import tpu as pltpu
from jax.sharding import PartitionSpec as P

HEAD_DIM = 128
GRID_W = 64
WIN_ROWS = 8
WIN_COLS = 16
REACH = WIN_ROWS // 2
EPS = 1e-06
LOG2E = 1.4426950408889634
MASKED = -1e30
VMEM_BYTES = 60 * 1024 * 1024


def dot32(a, b):
    return jnp.dot(a, b, preferred_element_type=jnp.float32)


def dot_t(a, b):
    return lax.dot_general(a, b, (((1,), (1,)), ((), ())), preferred_element_type=jnp.float32)


def divisor(count, most):
    return max(d for d in range(1, most + 1) if count % d == 0)


def normed_tokens(rows, gain):
    floats = rows.astype(jnp.float32)
    inverse = lax.rsqrt(jnp.mean(floats * floats, axis=-1, keepdims=True) + EPS)
    return floats * inverse * gain


def store_heads(out_ref, at, values, gain):
    count = values.shape[0]
    for h in range(values.shape[1] // HEAD_DIM):
        part = values[:, h * HEAD_DIM : (h + 1) * HEAD_DIM]
        part = part * lax.rsqrt(jnp.mean(part * part, axis=-1, keepdims=True) + EPS) * gain
        out_ref[pl.ds(at, count), h * HEAD_DIM : (h + 1) * HEAD_DIM] = part.astype(jnp.bfloat16)


def fill_bias(ob_ref, table, h):
    lane = lax.broadcasted_iota(jnp.int32, (GRID_W, 2 * GRID_W), 1)
    query = lax.broadcasted_iota(jnp.int32, (GRID_W, 2 * GRID_W), 0)
    key = lane % GRID_W
    begin = jnp.clip(query - WIN_COLS // 2, 0, GRID_W - WIN_COLS)
    valid = (key >= begin) & (key < begin + WIN_COLS)
    lanes = 2 * GRID_W
    for r in range(2 * WIN_ROWS - 2):
        low = jnp.broadcast_to(ob_ref[h, r : r + 1, :], (GRID_W, lanes))
        high = jnp.broadcast_to(ob_ref[h, r + 1 : r + 2, :], (GRID_W, lanes))
        low = pltpu.roll(low, lanes - (WIN_COLS - 1), 1, stride=1, stride_axis=0)
        high = pltpu.roll(high, GRID_W - (WIN_COLS - 1), 1, stride=1, stride_axis=0)
        both = jnp.where(lane < GRID_W, low, high) * LOG2E
        table[h, r] = jnp.where(valid, both, MASKED)


def layer_kernel(
    sp, tp, chunks, cb_ref, resid, cond, mshift, mscale, mgate, gain_ref, context, wq_hbm, wk_hbm,
    wv_hbm, qg, kg, ob_ref, wo_hbm, out_ref,
    tok, wq, wk, wv, wo, qbuf, kvbuf, ctxbuf, table, modsp, modtp, mods, att, full,
    load_sem, tok_send, pair_send, fwd_send, tok_recv, msp_send, msp_recv, mtp_send, mtp_recv,
    ctx_send, ctx_recv, halo_send, halo_recv, att_send, att_recv,
):
    me_s, me_t = lax.axis_index("sp"), lax.axis_index("tp")
    count, d = resid.shape
    chunk = count // chunks
    width = wq.shape[1]
    heads = width // HEAD_DIM
    tokens = count * tp
    rows = tokens // GRID_W
    total_rows = rows * sp
    first = me_s * rows
    chips = tp // 2
    chip, core = me_t // 2, me_t % 2
    pair = chip * 2 + (1 - core)

    def remote(src, dst, send, recv, axis, peer):
        return pltpu.make_async_remote_copy(
            src_ref=src, dst_ref=dst, send_sem=send, recv_sem=recv,
            device_id={axis: peer}, device_id_type=pl.DeviceIdType.MESH,
        )

    loads = [
        pltpu.make_async_copy(a, b, load_sem.at[i])
        for i, (a, b) in enumerate(
            ((wk_hbm, wk), (wv_hbm, wv), (wq_hbm, wq), (wo_hbm, wo), (resid, tok.at[me_t]))
        )
    ]
    for copy in (loads[4], loads[0], loads[1], loads[2]):
        copy.start()

    barrier = pltpu.get_barrier_semaphore()
    for k in range(1, sp):
        pl.semaphore_signal(
            barrier, inc=1, device_id={"sp": lax.rem(me_s + k, sp)},
            device_id_type=pl.DeviceIdType.MESH,
        )
    for k in range(1, tp):
        pl.semaphore_signal(
            barrier, inc=1, device_id={"tp": lax.rem(me_t + k, tp)},
            device_id_type=pl.DeviceIdType.MESH,
        )
    pl.semaphore_wait(barrier, sp + tp - 2)

    def part(block, c):
        return tok.at[block, pl.ds(pl.multiple_of(c * chunk, chunk), chunk), :]

    def mine(c):
        return resid.at[pl.ds(pl.multiple_of(c * chunk, chunk), chunk), :]

    def across(k, c):
        peer = lax.rem(chip + k, chips) * 2 + core
        return remote(
            mine(c), part(me_t, c), tok_send.at[(k - 1) * chunks + c],
            tok_recv.at[me_t * chunks + c], "tp", peer,
        )

    def beside(c):
        return remote(
            mine(c), part(me_t, c), pair_send.at[c], tok_recv.at[me_t * chunks + c], "tp", pair
        )

    def onward(k, c):
        block = lax.rem(chip + k, chips) * 2 + core
        return remote(
            part(block, c), part(block, c), fwd_send.at[(k - 1) * chunks + c],
            tok_recv.at[block * chunks + c], "tp", pair,
        )

    def arrived(block, c):
        remote(
            part(block, c), part(block, c), pair_send.at[0], tok_recv.at[block * chunks + c],
            "tp", pair,
        ).wait_recv()

    for k in range(1, chips):
        across(k, 0).start()
    for c in range(chunks):
        beside(c).start()

    lifted = cond[...].astype(jnp.float32)
    lifted = (lifted / (1.0 + jnp.exp(-lifted))).astype(jnp.bfloat16)
    lifted = jnp.broadcast_to(lifted, (16, lifted.shape[1]))
    for i, m in enumerate((mshift, mscale, mgate)):
        modsp[me_s, i : i + 1, :] = dot32(lifted, m[...])[0:1]
    modsp[me_s, 3:8, :] = jnp.zeros((5, modsp.shape[2]), jnp.float32)

    def to_sp(k, buf, send, recv):
        return remote(
            buf.at[me_s], buf.at[me_s], send.at[k - 1], recv.at[me_s], "sp", lax.rem(me_s + k, sp)
        )

    def from_sp(k, buf, send, recv):
        peer = lax.rem(me_s + k, sp)
        remote(buf.at[peer], buf.at[peer], send.at[k - 1], recv.at[peer], "sp", peer).wait_recv()

    for k in range(1, sp):
        to_sp(k, modsp, msp_send, msp_recv).start()

    loads[0].wait()
    loads[1].wait()
    normed = normed_tokens(context[...], gain_ref[...]).astype(jnp.bfloat16)
    own = ctxbuf.at[me_s]
    store_heads(own, 0, dot32(normed, wk[...]), kg[...])
    own[:, width:] = dot32(normed, wv[...]).astype(jnp.bfloat16)

    for k in range(1, sp):
        from_sp(k, modsp, msp_send, msp_recv)
    summed = modsp[0]
    for s in range(1, sp):
        summed = summed + modsp[s]
    modtp[me_t] = summed

    def to_tp(k):
        return remote(
            modtp.at[me_t], modtp.at[me_t], mtp_send.at[k - 1], mtp_recv.at[me_t], "tp",
            lax.rem(me_t + k, tp),
        )

    for k in range(1, tp):
        to_tp(k).start()
    for k in range(1, sp):
        to_sp(k, ctxbuf, ctx_send, ctx_recv).start()
    for c in range(1, chunks):
        for k in range(1, chips):
            across(k, c).start()
    def fill(h, carry):
        fill_bias(ob_ref, table, h)
        return carry

    lax.fori_loop(0, heads, fill, 0)

    loads[3].start()
    loads[2].wait()
    loads[4].wait()
    for k in range(1, tp):
        peer = lax.rem(me_t + k, tp)
        remote(
            modtp.at[peer], modtp.at[peer], mtp_send.at[k - 1], mtp_recv.at[peer], "tp", peer
        ).wait_recv()
    piece = modtp.shape[2]
    for t in range(tp):
        mods[:, t * piece : (t + 1) * piece] = modtp[t]

    edge = REACH * GRID_W

    def project(block, c):
        values = tok[block, pl.ds(pl.multiple_of(c * chunk, chunk), chunk), :]
        normed = normed_tokens(values, gain_ref[...]) * (1.0 + mods[1:2, :]) + mods[0:1, :]
        normed = normed.astype(jnp.bfloat16)
        at = pl.multiple_of(block * count + c * chunk, chunk)
        store_heads(qbuf, at, dot32(normed, wq[...]), qg[...])
        at = pl.multiple_of(edge + block * count + c * chunk, GRID_W)
        store_heads(kvbuf, at, dot32(normed, wk[...]), kg[...])
        kvbuf[pl.ds(at, chunk), width:] = dot32(normed, wv[...]).astype(jnp.bfloat16)

    def local_step(c, carry):
        project(me_t, c)
        return carry

    lax.fori_loop(0, chunks, local_step, 0)

    def pair_step(c, carry):
        arrived(pair, c)
        project(pair, c)
        return carry

    lax.fori_loop(0, chunks, pair_step, 0)

    def far_step(i, carry):
        c = i % chunks
        k = 1 + i // chunks
        near = lax.rem(chip + k, chips) * 2 + core
        other = lax.rem(chip + k, chips) * 2 + (1 - core)
        arrived(near, c)
        onward(k, c).start()
        project(near, c)
        arrived(other, c)
        project(other, c)
        return carry

    lax.fori_loop(0, (chips - 1) * chunks, far_step, 0)

    def up():
        return remote(
            kvbuf.at[pl.ds(edge, edge), :], kvbuf.at[pl.ds(edge + tokens, edge), :],
            halo_send.at[0], halo_recv.at[0], "sp", me_s - 1,
        )

    def down():
        return remote(
            kvbuf.at[pl.ds(tokens, edge), :], kvbuf.at[pl.ds(0, edge), :],
            halo_send.at[1], halo_recv.at[1], "sp", me_s + 1,
        )

    @pl.when(me_s > 0)
    def _():
        up().start()

    @pl.when(me_s < sp - 1)
    def _():
        down().start()

    for k in range(1, sp):
        from_sp(k, ctxbuf, ctx_send, ctx_recv)

    ctx_count = ctxbuf.shape[0] * ctxbuf.shape[1]
    factor = HEAD_DIM ** (-0.5) * LOG2E
    span = WIN_ROWS * GRID_W
    chunk_rows = rows // tp
    block = divisor(chunk_rows, 3)
    size = block * GRID_W

    def attend(dest, sub, h):
        lanes_k = pl.ds(pl.multiple_of(h * HEAD_DIM, HEAD_DIM), HEAD_DIM)
        lanes_v = pl.ds(pl.multiple_of(width + h * HEAD_DIM, HEAD_DIM), HEAD_DIM)
        row0 = dest * chunk_rows + sub * block
        queries = qbuf[pl.ds(pl.multiple_of(row0 * GRID_W, GRID_W), size), lanes_k]
        ctx_key = ctxbuf[:, :, lanes_k].reshape(ctx_count, HEAD_DIM)
        ctx_value = ctxbuf[:, :, lanes_v].reshape(ctx_count, HEAD_DIM)
        context_bias = cb_ref[h] * LOG2E
        s_ctx_all = dot_t(queries, ctx_key)
        p_ctx_all, outs, inverses = [], [], []
        for i in range(block):
            row = first + row0 + i
            start = jnp.clip(row - REACH, 0, total_rows - WIN_ROWS)
            r0 = start - row + WIN_ROWS - 1
            at = pl.multiple_of((start - first + REACH) * GRID_W, GRID_W)
            s_win = dot_t(queries[i * GRID_W : (i + 1) * GRID_W], kvbuf[pl.ds(at, span), lanes_k])
            bias = jnp.concatenate([table[h, r0 + 2 * m] for m in range(WIN_ROWS // 2)], axis=1)
            s_win = s_win * factor + bias
            s_ctx = s_ctx_all[i * GRID_W : (i + 1) * GRID_W] * factor + context_bias
            top = jnp.maximum(
                jnp.max(s_win, axis=1, keepdims=True), jnp.max(s_ctx, axis=1, keepdims=True)
            )
            e_win = jnp.exp2(s_win - top)
            e_ctx = jnp.exp2(s_ctx - top)
            total = jnp.sum(e_win, axis=1, keepdims=True) + jnp.sum(e_ctx, axis=1, keepdims=True)
            inverses.append(1.0 / total)
            p_ctx_all.append(e_ctx.astype(jnp.bfloat16))
            p_win = e_win.astype(jnp.bfloat16)
            outs.append(dot32(p_win, kvbuf[pl.ds(at, span), lanes_v]))
        out = jnp.concatenate(outs, axis=0)
        out = out + dot32(jnp.concatenate(p_ctx_all, axis=0), ctx_value)
        out = out * jnp.concatenate(inverses, axis=0)
        att[dest, pl.ds(pl.multiple_of(sub * size, size), size), lanes_k] = out.astype(jnp.bfloat16)

    def hand(dest):
        return remote(
            att.at[dest], full.at[me_t], att_send.at[dest], att_recv.at[me_t], "tp", dest
        )

    def position(i, carry):
        step = i // 2
        forward = tp // 2 + step - (i % 2) * (2 * step + 1)
        low = jnp.where(chip < (chips + 1) // 2, 1, 0)
        dest = low * forward + (1 - low) * (tp - 1 - forward)

        def unit(j, inner):
            attend(dest, j // heads, j % heads)
            return inner

        lax.fori_loop(0, chunk_rows // block * heads, unit, 0)

        @pl.when(dest != me_t)
        def _():
            hand(dest).start()

        return carry

    free = max(0, 2 * (tp // 2 - -(-REACH // chunk_rows)))
    lax.fori_loop(0, free, position, 0)

    @pl.when(me_s > 0)
    def _():
        down().wait_recv()

    @pl.when(me_s < sp - 1)
    def _():
        up().wait_recv()

    lax.fori_loop(free, tp, position, 0)

    full[me_t] = att[me_t]
    loads[3].wait()
    for k in range(1, tp):
        peer = lax.rem(me_t + k, tp)
        remote(
            att.at[peer], full.at[peer], att_send.at[peer], att_recv.at[peer], "tp", peer
        ).wait_recv()

    tile = HEAD_DIM * divisor(d // HEAD_DIM, 4)

    def finish(j, carry):
        lanes = pl.ds(pl.multiple_of(j * tile, tile), tile)
        result = dot32(full[0], wo[0:width, lanes])
        for t in range(1, tp):
            result = result + dot32(full[t], wo[t * width : (t + 1) * width, lanes])
        floats = tok[me_t, :, lanes].astype(jnp.float32)
        out_ref[:, lanes] = (floats + mods[2:3, lanes] * result).astype(jnp.bfloat16)
        return carry

    lax.fori_loop(0, d // tile, finish, 0)

    for c in range(chunks):
        beside(c).wait_send()
        for k in range(1, chips):
            across(k, c).wait_send()
            onward(k, c).wait_send()
    for k in range(1, sp):
        to_sp(k, modsp, msp_send, msp_recv).wait_send()
        to_sp(k, ctxbuf, ctx_send, ctx_recv).wait_send()
    for k in range(1, tp):
        to_tp(k).wait_send()
        hand(lax.rem(me_t + k, tp)).wait_send()

    @pl.when(me_s > 0)
    def _():
        up().wait_send()

    @pl.when(me_s < sp - 1)
    def _():
        down().wait_send()


def shards(
    resid,
    cond,
    mod_shift,
    mod_scale,
    mod_gate,
    norm_gain,
    context,
    w_query,
    w_key,
    w_value,
    query_gain,
    key_gain,
    offset_bias,
    context_bias,
    w_out,
):
    sp, tp = lax.axis_size("sp"), lax.axis_size("tp")
    count, d = resid.shape
    width = w_query.shape[1]
    heads = width // HEAD_DIM
    tokens = count * tp
    padded = jnp.pad(offset_bias, ((0, 0), (0, 1), (0, 2 * GRID_W - offset_bias.shape[2])))
    chunks = divisor(count // GRID_W, 3)
    chips = tp // 2
    bf, f32 = jnp.bfloat16, jnp.float32
    piece = mod_shift.shape[1]
    vmem = pl.BlockSpec(memory_space=pltpu.VMEM)
    hbm = pl.BlockSpec(memory_space=pl.ANY)
    sems = pltpu.SemaphoreType.DMA
    hops = max(1, (chips - 1) * chunks)
    return pl.pallas_call(
        functools.partial(layer_kernel, sp, tp, chunks),
        in_specs=[pl.BlockSpec(memory_space=pltpu.SMEM), hbm]
        + [vmem] * 6
        + [hbm] * 3
        + [vmem] * 3
        + [hbm],
        out_specs=vmem,
        out_shape=jax.ShapeDtypeStruct((count, d), bf),
        scratch_shapes=[
            pltpu.VMEM((tp, count, d), bf),
            pltpu.VMEM((d, width), bf),
            pltpu.VMEM((d, width), bf),
            pltpu.VMEM((d, width), bf),
            pltpu.VMEM((width * tp, d), bf),
            pltpu.VMEM((tokens, width), bf),
            pltpu.VMEM((tokens + 2 * REACH * GRID_W, 2 * width), bf),
            pltpu.VMEM((sp, context.shape[0], 2 * width), bf),
            pltpu.VMEM((heads, 2 * WIN_ROWS - 2, GRID_W, 2 * GRID_W), f32),
            pltpu.VMEM((sp, 8, piece), f32),
            pltpu.VMEM((tp, 8, piece), f32),
            pltpu.VMEM((8, d), f32),
            pltpu.VMEM((tp, count, width), bf),
            pltpu.VMEM((tp, count, width), bf),
            sems((5,)),
            sems((hops,)),
            sems((chunks,)),
            sems((hops,)),
            sems((tp * chunks,)),
            sems((sp,)),
            sems((sp,)),
            sems((tp,)),
            sems((tp,)),
            sems((sp,)),
            sems((sp,)),
            sems((2,)),
            sems((2,)),
            sems((tp,)),
            sems((tp,)),
        ],
        compiler_params=pltpu.CompilerParams(
            collective_id=0, has_side_effects=True, vmem_limit_bytes=VMEM_BYTES
        ),
        name="layer",
    )(
        context_bias, resid, cond[None, :], mod_shift, mod_scale, mod_gate, norm_gain[None, :],
        context, w_query, w_key, w_value, query_gain[None, :], key_gain[None, :], padded, w_out,
    )


def solution(mesh):
    in_specs = (
        P(("sp", "tp"), None),
        P("sp"),
        P("sp", "tp"),
        P("sp", "tp"),
        P("sp", "tp"),
        P(),
        P("sp", None),
        P(None, "tp"),
        P(None, "tp"),
        P(None, "tp"),
        P(),
        P(),
        P("tp", None, None),
        P("tp"),
        P(),
    )
    out_specs = P(("sp", "tp"), None)
    return jax.shard_map(shards, mesh=mesh, in_specs=in_specs, out_specs=out_specs, check_vma=False)
```

profile of v0, /device:TPU:4, one launch (start us, length us, event | category | flops | bytes accessed | tf_op | source)
XLA Modules:
  0.0 98.9 jit_solution(7796968069171103795)
XLA Ops:
  0.0 1.2 %broadcast_in_dim.12.cond = bf16[1,256]{1,0:T(2,128)(2,1)} reshape(bf16[256]{0:T(256)(128)(2,1)} %param.16) | data formatting | bytes 1024 | tf_op jit(solution)/shard_map/broadcast_in_dim | solution.py:468
  1.2 0.8 copy.16
  2.0 0.6 pad.4.ob_ref
  2.6 93.6 %layer.1 = bf16[384,2048]{1,0:T(8,128)(2,1)} custom-call(f32[4]{0:T(128)} %cb_ref.1, bf16[384,2048]{1,0:T(8,128)(2,1)} %resid.1, bf16[1,256]{1,0:T(2,128)(2,1)} %broadcast_in_dim.12.cond, bf16[256,512]{1,0:T(8,128)(2,1)} %mshift.1, bf16[256,512]{1,0:T(8,128)(2,1)} %mscale.1, bf16[256,512]{1,0:T(8,128)(2,1)} %mgate.1, f32[1,2048]{1,0:T(1,128)} %bitcast.3, ...), custom_call_target="tpu_custom_call" | custom-call | tf_op jit(solution)/shard_map/layer/pallas_call | solution.py:423
  96.2 2.7 %copy.18 = bf16[384,2048]{1,0:T(8,128)(2,1)} copy(bf16[384,2048]{1,0:T(8,128)(2,1)} %layer.1) | data formatting | bytes 3145728
where the time goes:
time: 99.1 us; the launch traced here: 98.9 us
  Pallas kernels  93.6 us (94%)
  local copies, waits for them, and re-layouts  5.33 us (5%)
    pallas_call x1, Pallas kernels, shards(): pl.pallas_call(functools.partial(layer_kernel, sp, tp, chunks), in_specs=...  93.6 us
    unnamed x2, local copies, waits for them, and re-layouts  3.48 us

commit v1 on v0

--- a/solution.py
+++ b/solution.py
@@ -45,25 +45,39 @@
 
 
 def fill_bias(ob_ref, table, h):
-    lane = lax.broadcasted_iota(jnp.int32, (GRID_W, 2 * GRID_W), 1)
-    query = lax.broadcasted_iota(jnp.int32, (GRID_W, 2 * GRID_W), 0)
-    key = lane % GRID_W
+    rows = 2 * WIN_ROWS - 1
+    lanes = 2 * GRID_W
+    lane = lax.broadcasted_iota(jnp.int32, (lanes, lanes), 1)
+    line = lax.broadcasted_iota(jnp.int32, (lanes, lanes), 0)
+    query = line % GRID_W
     begin = jnp.clip(query - WIN_COLS // 2, 0, GRID_W - WIN_COLS)
-    valid = (key >= begin) & (key < begin + WIN_COLS)
-    lanes = 2 * GRID_W
-    for r in range(2 * WIN_ROWS - 2):
-        low = jnp.broadcast_to(ob_ref[h, r : r + 1, :], (GRID_W, lanes))
-        high = jnp.broadcast_to(ob_ref[h, r + 1 : r + 2, :], (GRID_W, lanes))
-        low = pltpu.roll(low, lanes - (WIN_COLS - 1), 1, stride=1, stride_axis=0)
-        high = pltpu.roll(high, GRID_W - (WIN_COLS - 1), 1, stride=1, stride_axis=0)
-        both = jnp.where(lane < GRID_W, low, high) * LOG2E
-        table[h, r] = jnp.where(valid, both, MASKED)
+    valid = (lane >= begin) & (lane < begin + WIN_COLS)
+
+    def spread(r):
+        row = jnp.broadcast_to(ob_ref[r, pl.ds(h, 1), :], (GRID_W, lanes))
+        return pltpu.roll(row, lanes - (WIN_COLS - 1), 1, stride=1, stride_axis=0)
+
+    masked = jnp.full((GRID_W, lanes), MASKED, jnp.float32)
+
+    def put(slot, first, second):
+        both = jnp.concatenate([first, second], axis=0) * LOG2E
+        both = jnp.where(valid, both, MASKED)
+        table[h, slot] = both.T[:GRID_W]
+
+    low, high = REACH - 1, REACH - 1 + WIN_ROWS
+    spreads = [spread(r) for r in range(rows)]
+    for r in range(rows + 1):
+        put(r, spreads[r] if r < rows else masked, spreads[r - 1] if r > 0 else masked)
+    put(rows + 1, spreads[low], masked)
+    put(rows + 2, masked, spreads[high - 1])
+    table[h, rows + 3] = masked
 
 
 def layer_kernel(
     sp, tp, chunks, cb_ref, resid, cond, mshift, mscale, mgate, gain_ref, context, wq_hbm, wk_hbm,
-    wv_hbm, qg, kg, ob_ref, wo_hbm, out_ref,
-    tok, wq, wk, wv, wo, qbuf, kvbuf, ctxbuf, table, modsp, modtp, mods, att, full,
+    wv_hbm, qg, kg, ob_in, wo_hbm, out_ref,
+    tok, wq, wk, wv, wo, qbuf, kvbuf, ctxbuf, ob_ref, table, modsp, modtp, mods, att, full,
+    vt, ctxvt, score, prob,
     load_sem, tok_send, pair_send, fwd_send, tok_recv, msp_send, msp_recv, mtp_send, mtp_recv,
     ctx_send, ctx_recv, halo_send, halo_recv, att_send, att_recv,
 ):
@@ -139,16 +153,33 @@
             "tp", pair,
         ).wait_recv()
 
+    def order(i, side):
+        return i + side * (chunks - 1 - 2 * i)
+
+    def across_part(k, c, begin, size):
+        peer = lax.rem(chip + k, chips) * 2 + core
+        at = pl.ds(pl.multiple_of(c * chunk + begin, 16), size)
+        return remote(
+            resid.at[at, :], tok.at[me_t, at, :], tok_send.at[(k - 1) * chunks + c],
+            tok_recv.at[me_t * chunks + c], "tp", peer,
+        )
+
+    early = chunk // 4
+    first_chunk = order(0, core)
     for k in range(1, chips):
-        across(k, 0).start()
+        across_part(k, first_chunk, 0, early).start()
     for c in range(chunks):
         beside(c).start()
 
     lifted = cond[...].astype(jnp.float32)
     lifted = (lifted / (1.0 + jnp.exp(-lifted))).astype(jnp.bfloat16)
-    lifted = jnp.broadcast_to(lifted, (16, lifted.shape[1]))
+    lanes = lifted.shape[1]
     for i, m in enumerate((mshift, mscale, mgate)):
-        modsp[me_s, i : i + 1, :] = dot32(lifted, m[...])[0:1]
+        sums = []
+        for r in range(lifted.shape[0]):
+            line = jnp.broadcast_to(lifted[r : r + 1, :], (16, lanes))
+            sums.append(dot32(line, m[r * lanes : (r + 1) * lanes, :])[0:1])
+        modsp[me_s, i : i + 1, :] = functools.reduce(jnp.add, sums)
     modsp[me_s, 3:8, :] = jnp.zeros((5, modsp.shape[2]), jnp.float32)
 
     def to_sp(k, buf, send, recv):
@@ -185,11 +216,17 @@
 
     for k in range(1, tp):
         to_tp(k).start()
+    for k in range(1, chips):
+        across_part(k, first_chunk, early, chunk - early).start()
+    for i in range(1, chunks):
+        for k in range(1, chips):
+            across(k, order(i, core)).start()
     for k in range(1, sp):
         to_sp(k, ctxbuf, ctx_send, ctx_recv).start()
-    for c in range(1, chunks):
-        for k in range(1, chips):
-            across(k, c).start()
+
+    ob_ref[...] = jnp.zeros_like(ob_ref)
+    ob_ref[:, :, : ob_in.shape[2]] = ob_in[...]
+
     def fill(h, carry):
         fill_bias(ob_ref, table, h)
         return carry
@@ -233,140 +270,264 @@
 
     lax.fori_loop(0, chunks, pair_step, 0)
 
-    def far_step(i, carry):
-        c = i % chunks
-        k = 1 + i // chunks
+    def up():
+        return remote(
+            kvbuf.at[pl.ds(edge, edge), :], kvbuf.at[pl.ds(edge + tokens, edge), :],
+            halo_send.at[0], halo_recv.at[0], "sp", me_s - 1,
+        )
+
+    def down():
+        return remote(
+            kvbuf.at[pl.ds(tokens, edge), :], kvbuf.at[pl.ds(0, edge), :],
+            halo_send.at[1], halo_recv.at[1], "sp", me_s + 1,
+        )
+
+    upper = chip < (chips + 1) // 2
+    lower = jnp.logical_not(upper)
+
+    def send_up(when):
+        @pl.when(when & (me_s > 0))
+        def _():
+            up().start()
+
+    def send_down(when):
+        @pl.when(when & (me_s < sp - 1))
+        def _():
+            down().start()
+
+    @pl.when(me_s == 0)
+    def _():
+        kvbuf[0:edge, :] = jnp.zeros((edge, 2 * width), jnp.bfloat16)
+
+    @pl.when(me_s == sp - 1)
+    def _():
+        kvbuf[edge + tokens :, :] = jnp.zeros((edge, 2 * width), jnp.bfloat16)
+
+    ctx_count = ctxbuf.shape[0] * ctxbuf.shape[1]
+    factor = HEAD_DIM ** (-0.5) * LOG2E
+    span = edge
+    blocks = rows // REACH
+    half = 2 * GRID_W
+    keys = 3 * span
+    chunk_rows = rows // tp
+    piece_rows = divisor(chunk_rows, 2) if REACH % 2 == 0 else 1
+    piece = piece_rows * GRID_W
+    per_dest = chunk_rows // piece_rows
+    per_block = REACH // piece_rows
+    bias_rows = 2 * WIN_ROWS - 1
+    plain = list(range(bias_rows + 1))
+    lead, trail, blank = bias_rows + 1, bias_rows + 2, bias_rows + 3
+
+    def prepare(kb):
+        at = pl.ds(pl.multiple_of(kb * span, span), span)
+        vt[:, at] = kvbuf[at, width:].T
+
+    def prepare_context():
+        values = ctxbuf[:, :, width:].reshape(ctx_count, width)
+        ctxvt[...] = values.T
+
+    def tile_slot(line, side, first, last):
+        r = line + REACH - 1 - 2 * side
+        low, high = REACH - 1, REACH - 1 + WIN_ROWS
+        inner = lead if r == low else trail if r == high else r if low < r < high else blank
+        at_first = r if line >= REACH else blank
+        at_last = r if line < 2 * REACH else blank
+        if inner == at_first == at_last:
+            return inner
+        return inner + first * (at_first - inner) + last * (at_last - inner)
+
+    def attend(b, first, last):
+        at = pl.multiple_of(b * span, span)
+        heads = width // HEAD_DIM
+
+        def lanes_of(h, base):
+            return slice(base + h * HEAD_DIM, base + (h + 1) * HEAD_DIM)
+
+        def scores(h):
+            queries = qbuf[pl.ds(at, span), lanes_of(h, 0)]
+            slot = h % 2
+            tops = [jnp.full((8, half), MASKED, jnp.float32) for _ in range(2)]
+            for kb in range(3):
+                part = dot_t(kvbuf[pl.ds(at + kb * span, span), lanes_of(h, 0)], queries)
+                for i in range(REACH):
+                    line = kb * REACH + i
+                    for side in range(2):
+                        spot = tile_slot(line, side, first, last)
+                        if isinstance(spot, int) and spot == blank:
+                            continue
+                        cell = part[i * GRID_W : (i + 1) * GRID_W, side * half : (side + 1) * half]
+                        cell = cell * factor + table[h, spot]
+                        score[slot, line * GRID_W : (line + 1) * GRID_W, side * half : (side + 1) * half] = cell
+                        tops[side] = jnp.maximum(tops[side], jnp.max(cell.reshape(-1, 8, half), axis=0))
+            raw = jnp.full((8, 2 * half), -jnp.inf, jnp.float32)
+            for c in range(ctx_count // span):
+                ctx_key = ctxbuf[c * span // ctxbuf.shape[1] : (c + 1) * span // ctxbuf.shape[1], :, lanes_of(h, 0)]
+                part = dot_t(ctx_key.reshape(span, HEAD_DIM), queries)
+                score[slot, keys + c * span : keys + (c + 1) * span, :] = part
+                raw = jnp.maximum(raw, jnp.max(part.reshape(-1, 8, 2 * half), axis=0))
+            context_bias = cb_ref[h] * LOG2E
+            top = jnp.maximum(jnp.concatenate(tops, axis=1), raw * factor + context_bias)
+            return jnp.max(top, axis=0, keepdims=True), context_bias
+
+        def finish_head(h, top, context_bias):
+            slot = h % 2
+            totals = []
+            for side in range(2):
+                cols = slice(side * half, (side + 1) * half)
+                shift = jnp.broadcast_to(top[:, cols], (GRID_W, half))
+                total = jnp.zeros((8, half), jnp.float32)
+                for line in range(3 * REACH):
+                    span_rows = slice(line * GRID_W, (line + 1) * GRID_W)
+                    spot = tile_slot(line, side, first, last)
+                    if isinstance(spot, int) and spot == blank:
+                        prob[slot, span_rows, cols] = jnp.zeros((GRID_W, half), jnp.bfloat16)
+                        continue
+                    cell = jnp.exp2(score[slot, span_rows, cols] - shift)
+                    total = total + jnp.sum(cell.reshape(-1, 8, half), axis=0)
+                    prob[slot, span_rows, cols] = cell.astype(jnp.bfloat16)
+                shift = shift - context_bias
+                for c in range(ctx_count // GRID_W):
+                    span_rows = slice(keys + c * GRID_W, keys + (c + 1) * GRID_W)
+                    cell = jnp.exp2(score[slot, span_rows, cols] * factor - shift)
+                    total = total + jnp.sum(cell.reshape(-1, 8, half), axis=0)
+                    prob[slot, span_rows, cols] = cell.astype(jnp.bfloat16)
+                totals.append(jnp.sum(total, axis=0, keepdims=True))
+            out = dot32(vt[lanes_of(h, 0), pl.ds(at, keys)], prob[slot, :keys, :])
+            out = out + dot32(ctxvt[lanes_of(h, 0), :], prob[slot, keys:, :])
+            out = out * (1.0 / jnp.concatenate(totals, axis=1))
+            att[pl.ds(at, span), lanes_of(h, 0)] = out.T.astype(jnp.bfloat16)
+
+        state = scores(0)
+        for h in range(heads):
+            following = scores(h + 1) if h + 1 < heads else None
+            finish_head(h, *state)
+            state = following
+
+    def hand(p):
+        dest = p // per_dest
+        local = p % per_dest
+        src = pl.ds(pl.multiple_of(p * piece, piece), piece)
+        dst = pl.ds(pl.multiple_of(local * piece, piece), piece)
+        return remote(
+            att.at[src, :], full.at[me_t, dst, :], att_send.at[p],
+            att_recv.at[me_t * per_dest + local], "tp", dest,
+        )
+
+    def mirror(value, end):
+        return jnp.where(upper, value, end - value)
+
+    def attend_step(j, carry):
+        b = mirror(lax.rem(j + 1, blocks), blocks - 1)
+        fresh = mirror(lax.rem(j + 3, blocks + 2), blocks + 1)
+
+        @pl.when((b == 0) & (me_s > 0))
+        def _():
+            down().wait_recv()
+
+        @pl.when((b == blocks - 1) & (me_s < sp - 1))
+        def _():
+            up().wait_recv()
+
+        prepare(fresh)
+        first = jnp.where((b == 0) & (me_s == 0), 1, 0)
+        last = jnp.where((b == blocks - 1) & (me_s == sp - 1), 1, 0)
+        outer = first + last
+
+        @pl.when(outer == 0)
+        def _():
+            attend(b, 0, 0)
+
+        @pl.when(outer > 0)
+        def _():
+            attend(b, first, last)
+
+        for i in range(per_block):
+            p = b * per_block + i
+
+            @pl.when(p // per_dest != me_t)
+            def _():
+                hand(p).start()
+
+        return carry
+
+    def far(k, i):
         near = lax.rem(chip + k, chips) * 2 + core
         other = lax.rem(chip + k, chips) * 2 + (1 - core)
+        c = order(i, core)
         arrived(near, c)
         onward(k, c).start()
         project(near, c)
+        c = order(i, 1 - core)
         arrived(other, c)
         project(other, c)
+
+    send_early = chips == 2 and chunk_rows % 2 == 0 and chunks * piece_rows == chunk_rows
+    if send_early:
+        send_up(upper)
+        send_down(lower)
+        prepare(mirror(1, blocks + 1))
+        prepare(mirror(2, blocks + 1))
+
+        def overlap_step(i, carry):
+            far(1, i)
+
+            @pl.when(i == 0)
+            def _():
+                for k in range(1, sp):
+                    from_sp(k, ctxbuf, ctx_send, ctx_recv)
+                prepare_context()
+
+            send_down(upper & (i == chunks - 2))
+            send_up(lower & (i == chunks - 2))
+            end = i + 1 + (i // (chunks - 1)) * (blocks - chunks)
+            lax.fori_loop(i, end, attend_step, 0)
+            return carry
+
+        lax.fori_loop(0, chunks, overlap_step, 0)
+    else:
+        def far_step(i, carry):
+            far(1 + i // chunks, lax.rem(i, chunks))
+            return carry
+
+        lax.fori_loop(0, (chips - 1) * chunks, far_step, 0)
+        send_up(me_s >= 0)
+        send_down(me_s >= 0)
+        for k in range(1, sp):
+            from_sp(k, ctxbuf, ctx_send, ctx_recv)
+        prepare_context()
+        prepare(mirror(1, blocks + 1))
+        prepare(mirror(2, blocks + 1))
+        lax.fori_loop(0, blocks, attend_step, 0)
+
+    own = pl.ds(pl.multiple_of(me_t * count, count), count)
+    full[me_t] = att[own, :]
+    loads[3].wait()
+
+    tile = HEAD_DIM * divisor(d // HEAD_DIM, 4)
+
+    def finish(step, carry):
+        j = mirror(per_dest - 1 - step, per_dest - 1)
+        at = pl.ds(pl.multiple_of(j * piece, piece), piece)
+        for k in range(1, tp):
+            peer = lax.rem(me_t + k, tp)
+            remote(
+                full.at[peer, at, :], full.at[peer, at, :], att_send.at[0],
+                att_recv.at[peer * per_dest + j], "tp", peer,
+            ).wait_recv()
+
+        def column(n, inner):
+            lanes = pl.ds(pl.multiple_of(n * tile, tile), tile)
+            result = dot32(full[0, at, :], wo[0:width, lanes])
+            for t in range(1, tp):
+                result = result + dot32(full[t, at, :], wo[t * width : (t + 1) * width, lanes])
+            floats = tok[me_t, at, lanes].astype(jnp.float32)
+            out_ref[at, lanes] = (floats + mods[2:3, lanes] * result).astype(jnp.bfloat16)
+            return inner
+
+        lax.fori_loop(0, d // tile, column, 0)
         return carry
 
-    lax.fori_loop(0, (chips - 1) * chunks, far_step, 0)
-
-    def up():
-        return remote(
-            kvbuf.at[pl.ds(edge, edge), :], kvbuf.at[pl.ds(edge + tokens, edge), :],
-            halo_send.at[0], halo_recv.at[0], "sp", me_s - 1,
-        )
-
-    def down():
-        return remote(
-            kvbuf.at[pl.ds(tokens, edge), :], kvbuf.at[pl.ds(0, edge), :],
-            halo_send.at[1], halo_recv.at[1], "sp", me_s + 1,
-        )
-
-    @pl.when(me_s > 0)
-    def _():
-        up().start()
-
-    @pl.when(me_s < sp - 1)
-    def _():
-        down().start()
-
-    for k in range(1, sp):
-        from_sp(k, ctxbuf, ctx_send, ctx_recv)
-
-    ctx_count = ctxbuf.shape[0] * ctxbuf.shape[1]
-    factor = HEAD_DIM ** (-0.5) * LOG2E
-    span = WIN_ROWS * GRID_W
-    chunk_rows = rows // tp
-    block = divisor(chunk_rows, 3)
-    size = block * GRID_W
-
-    def attend(dest, sub, h):
-        lanes_k = pl.ds(pl.multiple_of(h * HEAD_DIM, HEAD_DIM), HEAD_DIM)
-        lanes_v = pl.ds(pl.multiple_of(width + h * HEAD_DIM, HEAD_DIM), HEAD_DIM)
-        row0 = dest * chunk_rows + sub * block
-        queries = qbuf[pl.ds(pl.multiple_of(row0 * GRID_W, GRID_W), size), lanes_k]
-        ctx_key = ctxbuf[:, :, lanes_k].reshape(ctx_count, HEAD_DIM)
-        ctx_value = ctxbuf[:, :, lanes_v].reshape(ctx_count, HEAD_DIM)
-        context_bias = cb_ref[h] * LOG2E
-        s_ctx_all = dot_t(queries, ctx_key)
-        p_ctx_all, outs, inverses = [], [], []
-        for i in range(block):
-            row = first + row0 + i
-            start = jnp.clip(row - REACH, 0, total_rows - WIN_ROWS)
-            r0 = start - row + WIN_ROWS - 1
-            at = pl.multiple_of((start - first + REACH) * GRID_W, GRID_W)
-            s_win = dot_t(queries[i * GRID_W : (i + 1) * GRID_W], kvbuf[pl.ds(at, span), lanes_k])
-            bias = jnp.concatenate([table[h, r0 + 2 * m] for m in range(WIN_ROWS // 2)], axis=1)
-            s_win = s_win * factor + bias
-            s_ctx = s_ctx_all[i * GRID_W : (i + 1) * GRID_W] * factor + context_bias
-            top = jnp.maximum(
-                jnp.max(s_win, axis=1, keepdims=True), jnp.max(s_ctx, axis=1, keepdims=True)
-            )
-            e_win = jnp.exp2(s_win - top)
-            e_ctx = jnp.exp2(s_ctx - top)
-            total = jnp.sum(e_win, axis=1, keepdims=True) + jnp.sum(e_ctx, axis=1, keepdims=True)
-            inverses.append(1.0 / total)
-            p_ctx_all.append(e_ctx.astype(jnp.bfloat16))
-            p_win = e_win.astype(jnp.bfloat16)
-            outs.append(dot32(p_win, kvbuf[pl.ds(at, span), lanes_v]))
-        out = jnp.concatenate(outs, axis=0)
-        out = out + dot32(jnp.concatenate(p_ctx_all, axis=0), ctx_value)
-        out = out * jnp.concatenate(inverses, axis=0)
-        att[dest, pl.ds(pl.multiple_of(sub * size, size), size), lanes_k] = out.astype(jnp.bfloat16)
-
-    def hand(dest):
-        return remote(
-            att.at[dest], full.at[me_t], att_send.at[dest], att_recv.at[me_t], "tp", dest
-        )
-
-    def position(i, carry):
-        step = i // 2
-        forward = tp // 2 + step - (i % 2) * (2 * step + 1)
-        low = jnp.where(chip < (chips + 1) // 2, 1, 0)
-        dest = low * forward + (1 - low) * (tp - 1 - forward)
-
-        def unit(j, inner):
-            attend(dest, j // heads, j % heads)
-            return inner
-
-        lax.fori_loop(0, chunk_rows // block * heads, unit, 0)
-
-        @pl.when(dest != me_t)
-        def _():
-            hand(dest).start()
-
-        return carry
-
-    free = max(0, 2 * (tp // 2 - -(-REACH // chunk_rows)))
-    lax.fori_loop(0, free, position, 0)
-
-    @pl.when(me_s > 0)
-    def _():
-        down().wait_recv()
-
-    @pl.when(me_s < sp - 1)
-    def _():
-        up().wait_recv()
-
-    lax.fori_loop(free, tp, position, 0)
-
-    full[me_t] = att[me_t]
-    loads[3].wait()
-    for k in range(1, tp):
-        peer = lax.rem(me_t + k, tp)
-        remote(
-            att.at[peer], full.at[peer], att_send.at[peer], att_recv.at[peer], "tp", peer
-        ).wait_recv()
-
-    tile = HEAD_DIM * divisor(d // HEAD_DIM, 4)
-
-    def finish(j, carry):
-        lanes = pl.ds(pl.multiple_of(j * tile, tile), tile)
-        result = dot32(full[0], wo[0:width, lanes])
-        for t in range(1, tp):
-            result = result + dot32(full[t], wo[t * width : (t + 1) * width, lanes])
-        floats = tok[me_t, :, lanes].astype(jnp.float32)
-        out_ref[:, lanes] = (floats + mods[2:3, lanes] * result).astype(jnp.bfloat16)
-        return carry
-
-    lax.fori_loop(0, d // tile, finish, 0)
+    lax.fori_loop(0, per_dest, finish, 0)
 
     for c in range(chunks):
         beside(c).wait_send()
@@ -378,7 +539,15 @@
         to_sp(k, ctxbuf, ctx_send, ctx_recv).wait_send()
     for k in range(1, tp):
         to_tp(k).wait_send()
-        hand(lax.rem(me_t + k, tp)).wait_send()
+
+    def sent(p, carry):
+        @pl.when(p // per_dest != me_t)
+        def _():
+            hand(p).wait_send()
+
+        return carry
+
+    lax.fori_loop(0, rows // piece_rows, sent, 0)
 
     @pl.when(me_s > 0)
     def _():
@@ -411,8 +580,12 @@
     width = w_query.shape[1]
     heads = width // HEAD_DIM
     tokens = count * tp
-    padded = jnp.pad(offset_bias, ((0, 0), (0, 1), (0, 2 * GRID_W - offset_bias.shape[2])))
-    chunks = divisor(count // GRID_W, 3)
+    lanes = min(cond.shape[0], HEAD_DIM)
+    chunk_rows = count // GRID_W
+    chunks = divisor(chunk_rows, 3)
+    pieces = chunk_rows // divisor(chunk_rows, 2)
+    ctx_count = context.shape[0] * sp
+    span = REACH * GRID_W
     chips = tp // 2
     bf, f32 = jnp.bfloat16, jnp.float32
     piece = mod_shift.shape[1]
@@ -438,12 +611,17 @@
             pltpu.VMEM((tokens, width), bf),
             pltpu.VMEM((tokens + 2 * REACH * GRID_W, 2 * width), bf),
             pltpu.VMEM((sp, context.shape[0], 2 * width), bf),
-            pltpu.VMEM((heads, 2 * WIN_ROWS - 2, GRID_W, 2 * GRID_W), f32),
+            pltpu.VMEM((offset_bias.shape[1], heads, 2 * GRID_W), f32),
+            pltpu.VMEM((heads, 2 * WIN_ROWS + 3, GRID_W, 2 * GRID_W), f32),
             pltpu.VMEM((sp, 8, piece), f32),
             pltpu.VMEM((tp, 8, piece), f32),
             pltpu.VMEM((8, d), f32),
+            pltpu.VMEM((tokens, width), bf),
             pltpu.VMEM((tp, count, width), bf),
-            pltpu.VMEM((tp, count, width), bf),
+            pltpu.VMEM((width, tokens + 2 * span), bf),
+            pltpu.VMEM((width, ctx_count), bf),
+            pltpu.VMEM((2, 3 * span + ctx_count, span), f32),
+            pltpu.VMEM((2, 3 * span + ctx_count, span), bf),
             sems((5,)),
             sems((hops,)),
             sems((chunks,)),
@@ -457,16 +635,17 @@
             sems((sp,)),
             sems((2,)),
             sems((2,)),
-            sems((tp,)),
-            sems((tp,)),
+            sems((tp * pieces,)),
+            sems((tp * pieces,)),
         ],
         compiler_params=pltpu.CompilerParams(
             collective_id=0, has_side_effects=True, vmem_limit_bytes=VMEM_BYTES
         ),
         name="layer",
     )(
-        context_bias, resid, cond[None, :], mod_shift, mod_scale, mod_gate, norm_gain[None, :],
-        context, w_query, w_key, w_value, query_gain[None, :], key_gain[None, :], padded, w_out,
+        context_bias, resid, cond.reshape(-1, lanes), mod_shift, mod_scale, mod_gate, norm_gain[None, :],
+        context, w_query, w_key, w_value, query_gain[None, :], key_gain[None, :],
+        jnp.transpose(offset_bias, (1, 0, 2)), w_out,
     )
 
 

time: 99.1 us -> 76.4 us (0.77)
  the two profiles are of different devices: /device:TPU:4 before, /device:TPU:0 now
where the time goes in v1:
time: 76.4 us; the launch traced here: 76.3 us
  Pallas kernels  73.5 us (96%)
  local copies, waits for them, and re-layouts  2.73 us (4%)
    pallas_call x1, Pallas kernels, shards(): pl.pallas_call(functools.partial(layer_kernel, sp, tp, chunks), in_specs=...  73.5 us
    unnamed x1, local copies, waits for them, and re-layouts  2.73 us

profile of v1, /device:TPU:0, one launch (start us, length us, event | category | flops | bytes accessed | tf_op | source)
XLA Modules:
  0.0 76.3 jit_solution(4130251123928797294)
XLA Ops:
  0.0 73.5 %layer.1 = bf16[384,2048]{1,0:T(8,128)(2,1)} custom-call(f32[4]{0:T(128)} %cb_ref.1, bf16[384,2048]{1,0:T(8,128)(2,1)} %resid.1, bf16[2,128]{1,0:T(2,128)(2,1)} %bitcast.7, bf16[256,512]{1,0:T(8,128)(2,1)} %mshift.1, bf16[256,512]{1,0:T(8,128)(2,1)} %mscale.1, bf16[256,512]{1,0:T(8,128)(2,1)} %mgate.1, f32[1,2048]{1,0:T(1,128)} %bitcast.6, ...), custom_call_target="tpu_custom_call" | custom-call | tf_op jit(solution)/shard_map/layer/pallas_call | solution.py:596
  73.6 2.7 %copy.17 = bf16[384,2048]{1,0:T(8,128)(2,1)} copy(bf16[384,2048]{1,0:T(8,128)(2,1)} %layer.1) | data formatting | bytes 3145728

commit v2 on v1

--- a/solution.py
+++ b/solution.py
@@ -15,7 +15,7 @@
 EPS = 1e-06
 LOG2E = 1.4426950408889634
 MASKED = -1e30
-VMEM_BYTES = 60 * 1024 * 1024
+VMEM_BYTES = 56 * 1024 * 1024
 
 
 def dot32(a, b):
@@ -74,10 +74,11 @@
 
 
 def layer_kernel(
-    sp, tp, chunks, cb_ref, resid, cond, mshift, mscale, mgate, gain_ref, context, wq_hbm, wk_hbm,
-    wv_hbm, qg, kg, ob_in, wo_hbm, out_ref,
+    sp, tp, chunks, cb_hbm, resid, cond_hbm, mshift_hbm, mscale_hbm, mgate_hbm, gain_hbm, context_hbm,
+    wq_hbm, wk_hbm, wv_hbm, qg_hbm, kg_hbm, ob_hbm, wo_hbm, out_ref,
+    cb, cond, mshift, mscale, mgate, gain_ref, context, qg, kg, ob_in,
     tok, wq, wk, wv, wo, qbuf, kvbuf, ctxbuf, ob_ref, table, modsp, modtp, mods, att, full,
-    vt, ctxvt, score, prob,
+    vt, ctxvt, score, prob, partial,
     load_sem, tok_send, pair_send, fwd_send, tok_recv, msp_send, msp_recv, mtp_send, mtp_recv,
     ctx_send, ctx_recv, halo_send, halo_recv, att_send, att_recv,
 ):
@@ -100,15 +101,6 @@
             device_id={axis: peer}, device_id_type=pl.DeviceIdType.MESH,
         )
 
-    loads = [
-        pltpu.make_async_copy(a, b, load_sem.at[i])
-        for i, (a, b) in enumerate(
-            ((wk_hbm, wk), (wv_hbm, wv), (wq_hbm, wq), (wo_hbm, wo), (resid, tok.at[me_t]))
-        )
-    ]
-    for copy in (loads[4], loads[0], loads[1], loads[2]):
-        copy.start()
-
     barrier = pltpu.get_barrier_semaphore()
     for k in range(1, sp):
         pl.semaphore_signal(
@@ -120,6 +112,26 @@
             barrier, inc=1, device_id={"tp": lax.rem(me_t + k, tp)},
             device_id_type=pl.DeviceIdType.MESH,
         )
+
+    def load(index, src, dst):
+        return pltpu.make_async_copy(src, dst, load_sem.at[index])
+
+    small = [
+        load(i, src, dst)
+        for i, (src, dst) in enumerate(
+            (
+                (cond_hbm, cond), (mshift_hbm, mshift), (mscale_hbm, mscale), (mgate_hbm, mgate),
+                (context_hbm, context), (gain_hbm, gain_ref), (kg_hbm, kg), (qg_hbm, qg),
+                (ob_hbm, ob_in), (cb_hbm, cb),
+            )
+        )
+    ]
+    base = len(small)
+    load_k, load_v = load(base, wk_hbm, wk), load(base + 1, wv_hbm, wv)
+    load_q, load_o = load(base + 2, wq_hbm, wq), load(base + 3, wo_hbm, wo)
+    load_tokens = load(base + 4, resid, tok.at[me_t])
+    for copy in small[:6] + [load_tokens, load_k, load_v] + small[6:] + [load_q]:
+        copy.start()
     pl.semaphore_wait(barrier, sp + tp - 2)
 
     def part(block, c):
@@ -128,10 +140,33 @@
     def mine(c):
         return resid.at[pl.ds(pl.multiple_of(c * chunk, chunk), chunk), :]
 
-    def across(k, c):
+    chunk_rows = rows // tp
+    weave = chips == 2 and chunks == 3 and chunk_rows == 6
+    is_low = chip // ((chips + 1) // 2)
+
+    def plan(i, side, low):
+        if not weave:
+            return 0, i
+        role = low * side + (1 - low) * (1 - side)
+        swap = jnp.where(i == 1 + role, 1, 0)
+        c = jnp.where(i == 0, chunks - 1, role)
+        return swap, low * c + (1 - low) * (chunks - 1 - c)
+
+    def across(k, i):
         peer = lax.rem(chip + k, chips) * 2 + core
-        return remote(
-            mine(c), part(me_t, c), tok_send.at[(k - 1) * chunks + c],
+        swap, c = plan(i, core, is_low)
+        owner = chip * 2 + (core + swap) % 2
+        return remote(
+            part(owner, c), part(owner, c), tok_send.at[(k - 1) * chunks + i],
+            tok_recv.at[owner * chunks + c], "tp", peer,
+        )
+
+    def across_part(k, begin, size, src):
+        peer = lax.rem(chip + k, chips) * 2 + core
+        c = plan(0, core, is_low)[1]
+        at = pl.ds(pl.multiple_of(c * chunk + begin, 16), size)
+        return remote(
+            src.at[at, :], tok.at[me_t, at, :], tok_send.at[(k - 1) * chunks],
             tok_recv.at[me_t * chunks + c], "tp", peer,
         )
 
@@ -140,10 +175,9 @@
             mine(c), part(me_t, c), pair_send.at[c], tok_recv.at[me_t * chunks + c], "tp", pair
         )
 
-    def onward(k, c):
-        block = lax.rem(chip + k, chips) * 2 + core
-        return remote(
-            part(block, c), part(block, c), fwd_send.at[(k - 1) * chunks + c],
+    def onward(k, i, block, c):
+        return remote(
+            part(block, c), part(block, c), fwd_send.at[(k - 1) * chunks + i],
             tok_recv.at[block * chunks + c], "tp", pair,
         )
 
@@ -153,24 +187,14 @@
             "tp", pair,
         ).wait_recv()
 
-    def order(i, side):
-        return i + side * (chunks - 1 - 2 * i)
-
-    def across_part(k, c, begin, size):
-        peer = lax.rem(chip + k, chips) * 2 + core
-        at = pl.ds(pl.multiple_of(c * chunk + begin, 16), size)
-        return remote(
-            resid.at[at, :], tok.at[me_t, at, :], tok_send.at[(k - 1) * chunks + c],
-            tok_recv.at[me_t * chunks + c], "tp", peer,
-        )
-
-    early = chunk // 4
-    first_chunk = order(0, core)
+    early = chunk * 3 // 128 * 16 if chunk >= 128 else chunk // 2
     for k in range(1, chips):
-        across_part(k, first_chunk, 0, early).start()
+        across_part(k, 0, early, resid).start()
     for c in range(chunks):
         beside(c).start()
 
+    for copy in small[:4]:
+        copy.wait()
     lifted = cond[...].astype(jnp.float32)
     lifted = (lifted / (1.0 + jnp.exp(-lifted))).astype(jnp.bfloat16)
     lanes = lifted.shape[1]
@@ -194,12 +218,27 @@
     for k in range(1, sp):
         to_sp(k, modsp, msp_send, msp_recv).start()
 
-    loads[0].wait()
-    loads[1].wait()
+    for copy in small[4:7]:
+        copy.wait()
+    load_k.wait()
+    load_v.wait()
     normed = normed_tokens(context[...], gain_ref[...]).astype(jnp.bfloat16)
     own = ctxbuf.at[me_s]
     store_heads(own, 0, dot32(normed, wk[...]), kg[...])
     own[:, width:] = dot32(normed, wv[...]).astype(jnp.bfloat16)
+    for k in range(1, sp):
+        to_sp(k, ctxbuf, ctx_send, ctx_recv).start()
+
+    for copy in small[7:]:
+        copy.wait()
+    ob_ref[...] = jnp.zeros_like(ob_ref)
+    ob_ref[:, :, : ob_in.shape[2]] = ob_in[...]
+
+    def fill(h, carry):
+        fill_bias(ob_ref, table, h)
+        return carry
+
+    lax.fori_loop(0, heads // 2, fill, 0)
 
     for k in range(1, sp):
         from_sp(k, modsp, msp_send, msp_recv)
@@ -216,26 +255,19 @@
 
     for k in range(1, tp):
         to_tp(k).start()
+    load_tokens.wait()
     for k in range(1, chips):
-        across_part(k, first_chunk, early, chunk - early).start()
+        across_part(k, early, chunk - early, tok.at[me_t]).start()
+    for c in range(chunks):
+        arrived(pair, c)
     for i in range(1, chunks):
         for k in range(1, chips):
-            across(k, order(i, core)).start()
-    for k in range(1, sp):
-        to_sp(k, ctxbuf, ctx_send, ctx_recv).start()
-
-    ob_ref[...] = jnp.zeros_like(ob_ref)
-    ob_ref[:, :, : ob_in.shape[2]] = ob_in[...]
-
-    def fill(h, carry):
-        fill_bias(ob_ref, table, h)
-        return carry
-
-    lax.fori_loop(0, heads, fill, 0)
-
-    loads[3].start()
-    loads[2].wait()
-    loads[4].wait()
+            across(k, i).start()
+
+    lax.fori_loop(heads // 2, heads, fill, 0)
+
+    load_o.start()
+    load_q.wait()
     for k in range(1, tp):
         peer = lax.rem(me_t + k, tp)
         remote(
@@ -264,7 +296,6 @@
     lax.fori_loop(0, chunks, local_step, 0)
 
     def pair_step(c, carry):
-        arrived(pair, c)
         project(pair, c)
         return carry
 
@@ -309,7 +340,6 @@
     blocks = rows // REACH
     half = 2 * GRID_W
     keys = 3 * span
-    chunk_rows = rows // tp
     piece_rows = divisor(chunk_rows, 2) if REACH % 2 == 0 else 1
     piece = piece_rows * GRID_W
     per_dest = chunk_rows // piece_rows
@@ -365,7 +395,7 @@
                 part = dot_t(ctx_key.reshape(span, HEAD_DIM), queries)
                 score[slot, keys + c * span : keys + (c + 1) * span, :] = part
                 raw = jnp.maximum(raw, jnp.max(part.reshape(-1, 8, 2 * half), axis=0))
-            context_bias = cb_ref[h] * LOG2E
+            context_bias = cb[0:1, h : h + 1] * LOG2E
             top = jnp.maximum(jnp.concatenate(tops, axis=1), raw * factor + context_bias)
             return jnp.max(top, axis=0, keepdims=True), context_bias
 
@@ -416,19 +446,17 @@
     def mirror(value, end):
         return jnp.where(upper, value, end - value)
 
-    def attend_step(j, carry):
-        b = mirror(lax.rem(j + 1, blocks), blocks - 1)
-        fresh = mirror(lax.rem(j + 3, blocks + 2), blocks + 1)
-
-        @pl.when((b == 0) & (me_s > 0))
+    def wait_top():
+        @pl.when(me_s > 0)
         def _():
             down().wait_recv()
 
-        @pl.when((b == blocks - 1) & (me_s < sp - 1))
+    def wait_bottom():
+        @pl.when(me_s < sp - 1)
         def _():
             up().wait_recv()
 
-        prepare(fresh)
+    def attend_block(b):
         first = jnp.where((b == 0) & (me_s == 0), 1, 0)
         last = jnp.where((b == blocks - 1) & (me_s == sp - 1), 1, 0)
         outer = first + last
@@ -442,84 +470,141 @@
             attend(b, first, last)
 
         for i in range(per_block):
-            p = b * per_block + i
+            p = b * per_block + jnp.where(upper, per_block - 1 - i, i)
 
             @pl.when(p // per_dest != me_t)
             def _():
                 hand(p).start()
 
-        return carry
-
     def far(k, i):
-        near = lax.rem(chip + k, chips) * 2 + core
-        other = lax.rem(chip + k, chips) * 2 + (1 - core)
-        c = order(i, core)
-        arrived(near, c)
-        onward(k, c).start()
-        project(near, c)
-        c = order(i, 1 - core)
-        arrived(other, c)
-        project(other, c)
-
-    send_early = chips == 2 and chunk_rows % 2 == 0 and chunks * piece_rows == chunk_rows
-    if send_early:
+        far_chip = lax.rem(chip + k, chips)
+        low = far_chip // ((chips + 1) // 2)
+        swap, c = plan(i, core, low)
+        block = far_chip * 2 + (core + swap) % 2
+        arrived(block, c)
+        onward(k, i, block, c).start()
+        project(block, c)
+        swap, c = plan(i, 1 - core, low)
+        block = far_chip * 2 + (1 - core + swap) % 2
+        arrived(block, c)
+        project(block, c)
+
+    def context_ready():
+        for k in range(1, sp):
+            from_sp(k, ctxbuf, ctx_send, ctx_recv)
+        prepare_context()
+
+    if weave:
         send_up(upper)
         send_down(lower)
         prepare(mirror(1, blocks + 1))
         prepare(mirror(2, blocks + 1))
 
-        def overlap_step(i, carry):
+        def attend_step(j, carry):
+            b = jnp.where(j == 0, 1, jnp.where(j == blocks - 1, 0, blocks - j))
+            fresh = jnp.where(j == 0, 3, jnp.where(j == 1, blocks + 1, jnp.where(j == 2, 4, 0)))
+            b = mirror(b, blocks - 1)
+
+            @pl.when(b == 0)
+            def _():
+                wait_top()
+
+            @pl.when(b == blocks - 1)
+            def _():
+                wait_bottom()
+
+            @pl.when((j < 3) | (j == blocks - 1))
+            def _():
+                prepare(mirror(fresh, blocks + 1))
+
+            attend_block(b)
+            return carry
+
+        def weave_step(i, carry):
             far(1, i)
 
             @pl.when(i == 0)
             def _():
-                for k in range(1, sp):
-                    from_sp(k, ctxbuf, ctx_send, ctx_recv)
-                prepare_context()
+                context_ready()
 
             send_down(upper & (i == chunks - 2))
             send_up(lower & (i == chunks - 2))
+
+            @pl.when(i == chunks - 2)
+            def _():
+                prepare(mirror(blocks - 1, blocks + 1))
+                prepare(mirror(blocks, blocks + 1))
+
             end = i + 1 + (i // (chunks - 1)) * (blocks - chunks)
             lax.fori_loop(i, end, attend_step, 0)
             return carry
 
-        lax.fori_loop(0, chunks, overlap_step, 0)
+        lax.fori_loop(0, chunks, weave_step, 0)
     else:
         def far_step(i, carry):
             far(1 + i // chunks, lax.rem(i, chunks))
             return carry
 
+        def prepare_step(kb, carry):
+            prepare(kb)
+            return carry
+
+        def plain_step(b, carry):
+            attend_block(b)
+            return carry
+
         lax.fori_loop(0, (chips - 1) * chunks, far_step, 0)
         send_up(me_s >= 0)
         send_down(me_s >= 0)
-        for k in range(1, sp):
-            from_sp(k, ctxbuf, ctx_send, ctx_recv)
-        prepare_context()
-        prepare(mirror(1, blocks + 1))
-        prepare(mirror(2, blocks + 1))
-        lax.fori_loop(0, blocks, attend_step, 0)
+        context_ready()
+        wait_top()
+        wait_bottom()
+        lax.fori_loop(0, blocks + 2, prepare_step, 0)
+        lax.fori_loop(0, blocks, plain_step, 0)
 
     own = pl.ds(pl.multiple_of(me_t * count, count), count)
     full[me_t] = att[own, :]
-    loads[3].wait()
+    load_o.wait()
 
     tile = HEAD_DIM * divisor(d // HEAD_DIM, 4)
 
-    def finish(step, carry):
+    def await_piece(peer, j):
+        at = pl.ds(pl.multiple_of(j * piece, piece), piece)
+        remote(
+            full.at[peer, at, :], full.at[peer, at, :], att_send.at[0],
+            att_recv.at[peer * per_dest + j], "tp", peer,
+        ).wait_recv()
+
+    def project_out(peer, at, lanes):
+        return dot32(full[peer, at, :], wo[pl.ds(pl.multiple_of(peer * width, width), width), lanes])
+
+    def near_piece(step, carry):
         j = mirror(per_dest - 1 - step, per_dest - 1)
         at = pl.ds(pl.multiple_of(j * piece, piece), piece)
-        for k in range(1, tp):
-            peer = lax.rem(me_t + k, tp)
-            remote(
-                full.at[peer, at, :], full.at[peer, at, :], att_send.at[0],
-                att_recv.at[peer * per_dest + j], "tp", peer,
-            ).wait_recv()
+        await_piece(pair, j)
 
         def column(n, inner):
             lanes = pl.ds(pl.multiple_of(n * tile, tile), tile)
-            result = dot32(full[0, at, :], wo[0:width, lanes])
-            for t in range(1, tp):
-                result = result + dot32(full[t, at, :], wo[t * width : (t + 1) * width, lanes])
+            partial[at, lanes] = project_out(me_t, at, lanes) + project_out(pair, at, lanes)
+            return inner
+
+        lax.fori_loop(0, d // tile, column, 0)
+        return carry
+
+    def far_piece(step, carry):
+        j = mirror(step, per_dest - 1)
+        at = pl.ds(pl.multiple_of(j * piece, piece), piece)
+        peers = [
+            lax.rem(chip + k, chips) * 2 + side for k in range(1, chips) for side in range(2)
+        ]
+        for peer in peers:
+            await_piece(peer, j)
+
+        def column(n, inner):
+            lanes = pl.ds(pl.multiple_of(n * tile, tile), tile)
+            result = partial[at, lanes]
+            for peer in peers:
+                result = result + project_out(peer, at, lanes)
             floats = tok[me_t, at, lanes].astype(jnp.float32)
             out_ref[at, lanes] = (floats + mods[2:3, lanes] * result).astype(jnp.bfloat16)
             return inner
@@ -527,13 +612,14 @@
         lax.fori_loop(0, d // tile, column, 0)
         return carry
 
-    lax.fori_loop(0, per_dest, finish, 0)
+    lax.fori_loop(0, per_dest, near_piece, 0)
+    lax.fori_loop(0, per_dest, far_piece, 0)
 
     for c in range(chunks):
         beside(c).wait_send()
         for k in range(1, chips):
             across(k, c).wait_send()
-            onward(k, c).wait_send()
+            onward(k, c, me_t, c).wait_send()
     for k in range(1, sp):
         to_sp(k, modsp, msp_send, msp_recv).wait_send()
         to_sp(k, ctxbuf, ctx_send, ctx_recv).wait_send()
@@ -590,19 +676,25 @@
     bf, f32 = jnp.bfloat16, jnp.float32
     piece = mod_shift.shape[1]
     vmem = pl.BlockSpec(memory_space=pltpu.VMEM)
-    hbm = pl.BlockSpec(memory_space=pl.ANY)
+    hbm = pl.BlockSpec(memory_space=pltpu.HBM)
     sems = pltpu.SemaphoreType.DMA
     hops = max(1, (chips - 1) * chunks)
     return pl.pallas_call(
         functools.partial(layer_kernel, sp, tp, chunks),
-        in_specs=[pl.BlockSpec(memory_space=pltpu.SMEM), hbm]
-        + [vmem] * 6
-        + [hbm] * 3
-        + [vmem] * 3
-        + [hbm],
+        in_specs=[hbm] * 15,
         out_specs=vmem,
-        out_shape=jax.ShapeDtypeStruct((count, d), bf),
+        out_shape=pltpu.VMEM((count, d), bf),
         scratch_shapes=[
+            pltpu.VMEM((1, heads), f32),
+            pltpu.VMEM((cond.shape[0] // lanes, lanes), bf),
+            pltpu.VMEM(mod_shift.shape, bf),
+            pltpu.VMEM(mod_scale.shape, bf),
+            pltpu.VMEM(mod_gate.shape, bf),
+            pltpu.VMEM((1, d), f32),
+            pltpu.VMEM(context.shape, bf),
+            pltpu.VMEM((1, HEAD_DIM), f32),
+            pltpu.VMEM((1, HEAD_DIM), f32),
+            pltpu.VMEM((offset_bias.shape[1], heads, offset_bias.shape[2]), f32),
             pltpu.VMEM((tp, count, d), bf),
             pltpu.VMEM((d, width), bf),
             pltpu.VMEM((d, width), bf),
@@ -622,7 +714,8 @@
             pltpu.VMEM((width, ctx_count), bf),
             pltpu.VMEM((2, 3 * span + ctx_count, span), f32),
             pltpu.VMEM((2, 3 * span + ctx_count, span), bf),
-            sems((5,)),
+            pltpu.VMEM((count, d), f32),
+            sems((15,)),
             sems((hops,)),
             sems((chunks,)),
             sems((hops,)),
@@ -643,7 +736,7 @@
         ),
         name="layer",
     )(
-        context_bias, resid, cond.reshape(-1, lanes), mod_shift, mod_scale, mod_gate, norm_gain[None, :],
+        context_bias[None, :], resid, cond.reshape(-1, lanes), mod_shift, mod_scale, mod_gate, norm_gain[None, :],
         context, w_query, w_key, w_value, query_gain[None, :], key_gain[None, :],
         jnp.transpose(offset_bias, (1, 0, 2)), w_out,
     )

time: 76.4 us -> 80.4 us (1.052)
  the two profiles are of different devices: /device:TPU:0 before, /device:TPU:9 now
where the time goes in v2:
time: 80.4 us; the launch traced here: 80.2 us
  Pallas kernels  79.1 us (98%)
  local copies, waits for them, and re-layouts  1.15 us (1%)
    pallas_call x1, Pallas kernels, shards(): pl.pallas_call(functools.partial(layer_kernel, sp, tp, chunks), in_specs=...  79.1 us

profile of v2, /device:TPU:9, one launch (start us, length us, event | category | flops | bytes accessed | tf_op | source)
XLA Modules:
  0.0 80.2 jit_solution(12890117724347799879)
XLA Ops:
  0.0 79.1 %layer.1 = bf16[384,2048]{1,0:T(8,128)(2,1)S(1)} custom-call(f32[1,4]{1,0:T(1,128)} %bitcast.8, bf16[384,2048]{1,0:T(8,128)(2,1)} %resid.1, bf16[2,128]{1,0:T(2,128)(2,1)} %bitcast.9, bf16[256,512]{1,0:T(8,128)(2,1)} %mshift_hbm.1, bf16[256,512]{1,0:T(8,128)(2,1)} %mscale_hbm.1, bf16[256,512]{1,0:T(8,128)(2,1)} %mgate_hbm.1, f32[1,2048]{1,0:T(1,128)} %bitcast.7, ...), custom_call_target="tpu_custom_call" | custom-call | tf_op jit(solution)/shard_map/layer/pallas_call | solution.py:682
  79.1 1.1 %copy.17 = bf16[384,2048]{1,0:T(8,128)(2,1)} copy(bf16[384,2048]{1,0:T(8,128)(2,1)S(1)} %layer.1) | data formatting | bytes 3145728

commit v3 on v2

--- a/solution.py
+++ b/solution.py
@@ -142,19 +142,15 @@
 
     chunk_rows = rows // tp
     weave = chips == 2 and chunks == 3 and chunk_rows == 6
-    is_low = chip // ((chips + 1) // 2)
-
-    def plan(i, side, low):
+
+    def plan(i, side):
         if not weave:
             return 0, i
-        role = low * side + (1 - low) * (1 - side)
-        swap = jnp.where(i == 1 + role, 1, 0)
-        c = jnp.where(i == 0, chunks - 1, role)
-        return swap, low * c + (1 - low) * (chunks - 1 - c)
+        return jnp.where(i == 1 + side, 1, 0), jnp.where(i == 0, chunks - 1, side)
 
     def across(k, i):
         peer = lax.rem(chip + k, chips) * 2 + core
-        swap, c = plan(i, core, is_low)
+        swap, c = plan(i, core)
         owner = chip * 2 + (core + swap) % 2
         return remote(
             part(owner, c), part(owner, c), tok_send.at[(k - 1) * chunks + i],
@@ -163,7 +159,7 @@
 
     def across_part(k, begin, size, src):
         peer = lax.rem(chip + k, chips) * 2 + core
-        c = plan(0, core, is_low)[1]
+        c = plan(0, core)[1]
         at = pl.ds(pl.multiple_of(c * chunk + begin, 16), size)
         return remote(
             src.at[at, :], tok.at[me_t, at, :], tok_send.at[(k - 1) * chunks],
@@ -226,8 +222,6 @@
     own = ctxbuf.at[me_s]
     store_heads(own, 0, dot32(normed, wk[...]), kg[...])
     own[:, width:] = dot32(normed, wv[...]).astype(jnp.bfloat16)
-    for k in range(1, sp):
-        to_sp(k, ctxbuf, ctx_send, ctx_recv).start()
 
     for copy in small[7:]:
         copy.wait()
@@ -264,6 +258,29 @@
         for k in range(1, chips):
             across(k, i).start()
 
+    twin = me_s + 1 - 2 * (me_s % 2)
+    steps = sp // 2
+
+    def context_copy(block, peer, index):
+        return remote(
+            ctxbuf.at[block], ctxbuf.at[block], ctx_send.at[index], ctx_recv.at[block], "sp", peer
+        )
+
+    def fellow(m):
+        return lax.rem(me_s + 2 * (m // 2 + 1 if m % 2 == 0 else steps - m // 2 - 1), sp)
+
+    def context_arrived(block):
+        context_copy(block, twin, 0).wait_recv()
+
+    context_copy(me_s, twin, 0).start()
+    for m in range(steps - 1):
+        context_copy(me_s, fellow(m), 1 + m).start()
+
+    def pass_context(begin, end):
+        for m in range(begin, end):
+            context_arrived(fellow(m))
+            context_copy(fellow(m), twin, steps + m).start()
+
     lax.fori_loop(heads // 2, heads, fill, 0)
 
     load_o.start()
@@ -294,16 +311,21 @@
         return carry
 
     lax.fori_loop(0, chunks, local_step, 0)
+    near = min(2, steps - 1)
+    pass_context(0, near)
 
     def pair_step(c, carry):
         project(pair, c)
         return carry
 
     lax.fori_loop(0, chunks, pair_step, 0)
+    pass_context(near, steps - 1)
+
+    ahead = (WIN_ROWS - REACH - 1) * GRID_W
 
     def up():
         return remote(
-            kvbuf.at[pl.ds(edge, edge), :], kvbuf.at[pl.ds(edge + tokens, edge), :],
+            kvbuf.at[pl.ds(edge, ahead), :], kvbuf.at[pl.ds(edge + tokens, ahead), :],
             halo_send.at[0], halo_recv.at[0], "sp", me_s - 1,
         )
 
@@ -330,9 +352,11 @@
     def _():
         kvbuf[0:edge, :] = jnp.zeros((edge, 2 * width), jnp.bfloat16)
 
+    kvbuf[edge + tokens + ahead :, :] = jnp.zeros((edge - ahead, 2 * width), jnp.bfloat16)
+
     @pl.when(me_s == sp - 1)
     def _():
-        kvbuf[edge + tokens :, :] = jnp.zeros((edge, 2 * width), jnp.bfloat16)
+        kvbuf[edge + tokens : edge + tokens + ahead, :] = jnp.zeros((ahead, 2 * width), jnp.bfloat16)
 
     ctx_count = ctxbuf.shape[0] * ctxbuf.shape[1]
     factor = HEAD_DIM ** (-0.5) * LOG2E
@@ -443,8 +467,11 @@
             att_recv.at[me_t * per_dest + local], "tp", dest,
         )
 
-    def mirror(value, end):
-        return jnp.where(upper, value, end - value)
+    def choose(index, for_upper, for_lower):
+        value = 0
+        for at, (a, b) in enumerate(zip(for_upper, for_lower)):
+            value = value + jnp.where(index == at, jnp.where(upper, a, b), 0)
+        return value
 
     def wait_top():
         @pl.when(me_s > 0)
@@ -470,7 +497,7 @@
             attend(b, first, last)
 
         for i in range(per_block):
-            p = b * per_block + jnp.where(upper, per_block - 1 - i, i)
+            p = b * per_block + per_block - 1 - i
 
             @pl.when(p // per_dest != me_t)
             def _():
@@ -478,65 +505,65 @@
 
     def far(k, i):
         far_chip = lax.rem(chip + k, chips)
-        low = far_chip // ((chips + 1) // 2)
-        swap, c = plan(i, core, low)
+        swap, c = plan(i, core)
         block = far_chip * 2 + (core + swap) % 2
         arrived(block, c)
         onward(k, i, block, c).start()
         project(block, c)
-        swap, c = plan(i, 1 - core, low)
+        swap, c = plan(i, 1 - core)
         block = far_chip * 2 + (1 - core + swap) % 2
         arrived(block, c)
         project(block, c)
 
     def context_ready():
-        for k in range(1, sp):
-            from_sp(k, ctxbuf, ctx_send, ctx_recv)
+        context_arrived(twin)
+        for m in range(1, steps):
+            context_arrived(lax.rem(twin + 2 * m, sp))
         prepare_context()
 
     if weave:
         send_up(upper)
-        send_down(lower)
-        prepare(mirror(1, blocks + 1))
-        prepare(mirror(2, blocks + 1))
+
+        def prepare_all(for_upper, for_lower):
+            for a, b in zip(for_upper, for_lower):
+                prepare(jnp.where(upper, a, b))
+
+        prepare_all((1, 2, 3), (4, 5, 6))
 
         def attend_step(j, carry):
-            b = jnp.where(j == 0, 1, jnp.where(j == blocks - 1, 0, blocks - j))
-            fresh = jnp.where(j == 0, 3, jnp.where(j == 1, blocks + 1, jnp.where(j == 2, 4, 0)))
-            b = mirror(b, blocks - 1)
+            b = choose(j, (1, 5, 4, 3, 2, 0), (2, 4, 3, 1, 0, 5))
 
             @pl.when(b == 0)
             def _():
                 wait_top()
+                prepare(0)
 
             @pl.when(b == blocks - 1)
             def _():
                 wait_bottom()
-
-            @pl.when((j < 3) | (j == blocks - 1))
-            def _():
-                prepare(mirror(fresh, blocks + 1))
+                prepare(blocks + 1)
 
             attend_block(b)
             return carry
 
         def weave_step(i, carry):
             far(1, i)
-
-            @pl.when(i == 0)
+            send_down((lower & (i == 0)) | (upper & (i == 1)))
+            send_up(lower & (i == 2))
+
+            @pl.when(i == 1)
             def _():
                 context_ready()
-
-            send_down(upper & (i == chunks - 2))
-            send_up(lower & (i == chunks - 2))
-
-            @pl.when(i == chunks - 2)
+                prepare_all((5, 6), (2, 3))
+
+            @pl.when(i == 2)
             def _():
-                prepare(mirror(blocks - 1, blocks + 1))
-                prepare(mirror(blocks, blocks + 1))
-
-            end = i + 1 + (i // (chunks - 1)) * (blocks - chunks)
-            lax.fori_loop(i, end, attend_step, 0)
+                prepare_all((4,), (1,))
+
+            middle = jnp.where(upper, 2, 3)
+            begin = jnp.where(i == 2, middle, 0)
+            end = jnp.where(i == 0, 0, jnp.where(i == 2, blocks, middle))
+            lax.fori_loop(begin, end, attend_step, 0)
             return carry
 
         lax.fori_loop(0, chunks, weave_step, 0)
@@ -578,21 +605,18 @@
     def project_out(peer, at, lanes):
         return dot32(full[peer, at, :], wo[pl.ds(pl.multiple_of(peer * width, width), width), lanes])
 
-    def near_piece(step, carry):
-        j = mirror(per_dest - 1 - step, per_dest - 1)
-        at = pl.ds(pl.multiple_of(j * piece, piece), piece)
+    for j in range(per_dest):
         await_piece(pair, j)
 
-        def column(n, inner):
-            lanes = pl.ds(pl.multiple_of(n * tile, tile), tile)
-            partial[at, lanes] = project_out(me_t, at, lanes) + project_out(pair, at, lanes)
-            return inner
-
-        lax.fori_loop(0, d // tile, column, 0)
+    def near_column(n, carry):
+        lanes = pl.ds(pl.multiple_of(n * tile, tile), tile)
+        partial[:, lanes] = project_out(me_t, slice(None), lanes) + project_out(pair, slice(None), lanes)
         return carry
 
+    lax.fori_loop(0, d // tile, near_column, 0, unroll=True)
+
     def far_piece(step, carry):
-        j = mirror(step, per_dest - 1)
+        j = per_dest - 1 - step
         at = pl.ds(pl.multiple_of(j * piece, piece), piece)
         peers = [
             lax.rem(chip + k, chips) * 2 + side for k in range(1, chips) for side in range(2)
@@ -609,10 +633,9 @@
             out_ref[at, lanes] = (floats + mods[2:3, lanes] * result).astype(jnp.bfloat16)
             return inner
 
-        lax.fori_loop(0, d // tile, column, 0)
+        lax.fori_loop(0, d // tile, column, 0, unroll=True)
         return carry
 
-    lax.fori_loop(0, per_dest, near_piece, 0)
     lax.fori_loop(0, per_dest, far_piece, 0)
 
     for c in range(chunks):
@@ -622,7 +645,10 @@
             onward(k, c, me_t, c).wait_send()
     for k in range(1, sp):
         to_sp(k, modsp, msp_send, msp_recv).wait_send()
-        to_sp(k, ctxbuf, ctx_send, ctx_recv).wait_send()
+    context_copy(me_s, twin, 0).wait_send()
+    for m in range(steps - 1):
+        context_copy(me_s, twin, 1 + m).wait_send()
+        context_copy(me_s, twin, steps + m).wait_send()
     for k in range(1, tp):
         to_tp(k).wait_send()
 

time: 80.4 us -> 64.9 us (0.81)
  the two profiles are of different devices: /device:TPU:9 before, /device:TPU:0 now
where the time goes in v3:
time: 64.9 us; the launch traced here: 64.8 us
  Pallas kernels  63.6 us (98%)
  local copies, waits for them, and re-layouts  1.15 us (2%)
    pallas_call x1, Pallas kernels, shards(): pl.pallas_call(functools.partial(layer_kernel, sp, tp, chunks), in_specs=...  63.6 us

profile of v3, /device:TPU:0, one launch (start us, length us, event | category | flops | bytes accessed | tf_op | source)
XLA Modules:
  0.0 64.8 jit_solution(16901433800463969038)
XLA Ops:
  0.0 63.6 %layer.1 = bf16[384,2048]{1,0:T(8,128)(2,1)S(1)} custom-call(f32[1,4]{1,0:T(1,128)} %bitcast.8, bf16[384,2048]{1,0:T(8,128)(2,1)} %resid.1, bf16[2,128]{1,0:T(2,128)(2,1)} %bitcast.9, bf16[256,512]{1,0:T(8,128)(2,1)} %mshift_hbm.1, bf16[256,512]{1,0:T(8,128)(2,1)} %mscale_hbm.1, bf16[256,512]{1,0:T(8,128)(2,1)} %mgate_hbm.1, f32[1,2048]{1,0:T(1,128)} %bitcast.7, ...), custom_call_target="tpu_custom_call" | custom-call | tf_op jit(solution)/shard_map/layer/pallas_call | solution.py:708
  63.7 1.1 %copy.17 = bf16[384,2048]{1,0:T(8,128)(2,1)} copy(bf16[384,2048]{1,0:T(8,128)(2,1)S(1)} %layer.1) | data formatting | bytes 3145728

commit v4 on v3

--- a/solution.py
+++ b/solution.py
@@ -496,6 +496,7 @@
         def _():
             attend(b, first, last)
 
+    def hand_block(b):
         for i in range(per_block):
             p = b * per_block + per_block - 1 - i
 
@@ -503,12 +504,14 @@
             def _():
                 hand(p).start()
 
-    def far(k, i):
+    def far(k, i, on_arrival=None):
         far_chip = lax.rem(chip + k, chips)
         swap, c = plan(i, core)
         block = far_chip * 2 + (core + swap) % 2
         arrived(block, c)
         onward(k, i, block, c).start()
+        if on_arrival is not None:
+            on_arrival()
         project(block, c)
         swap, c = plan(i, 1 - core)
         block = far_chip * 2 + (1 - core + swap) % 2
@@ -531,7 +534,7 @@
         prepare_all((1, 2, 3), (4, 5, 6))
 
         def attend_step(j, carry):
-            b = choose(j, (1, 5, 4, 3, 2, 0), (2, 4, 3, 1, 0, 5))
+            b = choose(j, (1, 5, 4, 3, 2, 0), (4, 2, 1, 0, 3, 5))
 
             @pl.when(b == 0)
             def _():
@@ -544,10 +547,22 @@
                 prepare(blocks + 1)
 
             attend_block(b)
+
+            @pl.when(b != early_block)
+            def _():
+                hand_block(b)
+
             return carry
 
+        early_block = jnp.where(upper, 5, 2)
+
         def weave_step(i, carry):
-            far(1, i)
+            def hand_early():
+                @pl.when(i == 2)
+                def _():
+                    hand_block(early_block)
+
+            far(1, i, hand_early)
             send_down((lower & (i == 0)) | (upper & (i == 1)))
             send_up(lower & (i == 2))
 
@@ -560,9 +575,8 @@
             def _():
                 prepare_all((4,), (1,))
 
-            middle = jnp.where(upper, 2, 3)
-            begin = jnp.where(i == 2, middle, 0)
-            end = jnp.where(i == 0, 0, jnp.where(i == 2, blocks, middle))
+            begin = jnp.where(i == 2, 2, 0)
+            end = jnp.where(i == 0, 0, jnp.where(i == 2, blocks, 2))
             lax.fori_loop(begin, end, attend_step, 0)
             return carry
 
@@ -578,6 +592,7 @@
 
         def plain_step(b, carry):
             attend_block(b)
+            hand_block(b)
             return carry
 
         lax.fori_loop(0, (chips - 1) * chunks, far_step, 0)

time: 64.9 us -> 64 us (0.986)
  Pallas kernels: 63.6 us -> 62.7 us
    pallas_call x1, Pallas kernels: 63.6 us -> 62.7 us  [shards(): pl.pallas_call(functools.partial(layer_kernel, sp, tp, chunks), in_specs=...]
where the time goes in v4:
time: 64 us; the launch traced here: 63.8 us
  Pallas kernels  62.7 us (98%)
  local copies, waits for them, and re-layouts  1.15 us (2%)
    pallas_call x1, Pallas kernels, shards(): pl.pallas_call(functools.partial(layer_kernel, sp, tp, chunks), in_specs=...  62.7 us

profile of v4, /device:TPU:0, one launch (start us, length us, event | category | flops | bytes accessed | tf_op | source)
XLA Modules:
  0.0 63.8 jit_solution(3566950827180451472)
XLA Ops:
  0.0 62.7 %layer.1 = bf16[384,2048]{1,0:T(8,128)(2,1)S(1)} custom-call(f32[1,4]{1,0:T(1,128)} %bitcast.8, bf16[384,2048]{1,0:T(8,128)(2,1)} %resid.1, bf16[2,128]{1,0:T(2,128)(2,1)} %bitcast.9, bf16[256,512]{1,0:T(8,128)(2,1)} %mshift_hbm.1, bf16[256,512]{1,0:T(8,128)(2,1)} %mscale_hbm.1, bf16[256,512]{1,0:T(8,128)(2,1)} %mgate_hbm.1, f32[1,2048]{1,0:T(1,128)} %bitcast.7, ...), custom_call_target="tpu_custom_call" | custom-call | tf_op jit(solution)/shard_map/layer/pallas_call | solution.py:723
  62.7 1.1 %copy.17 = bf16[384,2048]{1,0:T(8,128)(2,1)} copy(bf16[384,2048]{1,0:T(8,128)(2,1)S(1)} %layer.1) | data formatting | bytes 3145728

commit v5 on v4

--- a/solution.py
+++ b/solution.py
@@ -148,13 +148,16 @@
             return 0, i
         return jnp.where(i == 1 + side, 1, 0), jnp.where(i == 0, chunks - 1, side)
 
+    def slot_of(block, at_chip, c):
+        return 1 + (lax.rem(block - 2 * at_chip + tp, tp) - 2) * chunks + c
+
     def across(k, i):
         peer = lax.rem(chip + k, chips) * 2 + core
         swap, c = plan(i, core)
         owner = chip * 2 + (core + swap) % 2
         return remote(
-            part(owner, c), part(owner, c), tok_send.at[(k - 1) * chunks + i],
-            tok_recv.at[owner * chunks + c], "tp", peer,
+            part(owner, c), part(owner, c), tok_send.at[0],
+            tok_recv.at[slot_of(owner, lax.rem(chip + k, chips), c)], "tp", peer,
         )
 
     def across_part(k, begin, size, src):
@@ -162,24 +165,27 @@
         c = plan(0, core)[1]
         at = pl.ds(pl.multiple_of(c * chunk + begin, 16), size)
         return remote(
-            src.at[at, :], tok.at[me_t, at, :], tok_send.at[(k - 1) * chunks],
-            tok_recv.at[me_t * chunks + c], "tp", peer,
+            src.at[at, :], tok.at[me_t, at, :], tok_send.at[0],
+            tok_recv.at[slot_of(me_t, lax.rem(chip + k, chips), c)], "tp", peer,
         )
 
     def beside(c):
         return remote(
-            mine(c), part(me_t, c), pair_send.at[c], tok_recv.at[me_t * chunks + c], "tp", pair
-        )
-
-    def onward(k, i, block, c):
-        return remote(
-            part(block, c), part(block, c), fwd_send.at[(k - 1) * chunks + i],
-            tok_recv.at[block * chunks + c], "tp", pair,
-        )
+            mine(c), part(me_t, c), pair_send.at[0], tok_recv.at[0], "tp", pair
+        )
+
+    def onward(block, c):
+        return remote(
+            part(block, c), part(block, c), fwd_send.at[0],
+            tok_recv.at[slot_of(block, chip, c)], "tp", pair,
+        )
+
+    def whole(ref, send, recv, axis, peer):
+        return remote(ref, ref, send.at[0], recv.at[0], axis, peer)
 
     def arrived(block, c):
         remote(
-            part(block, c), part(block, c), pair_send.at[0], tok_recv.at[block * chunks + c],
+            part(block, c), part(block, c), pair_send.at[0], tok_recv.at[slot_of(block, chip, c)],
             "tp", pair,
         ).wait_recv()
 
@@ -202,17 +208,19 @@
         modsp[me_s, i : i + 1, :] = functools.reduce(jnp.add, sums)
     modsp[me_s, 3:8, :] = jnp.zeros((5, modsp.shape[2]), jnp.float32)
 
-    def to_sp(k, buf, send, recv):
-        return remote(
-            buf.at[me_s], buf.at[me_s], send.at[k - 1], recv.at[me_s], "sp", lax.rem(me_s + k, sp)
-        )
-
-    def from_sp(k, buf, send, recv):
-        peer = lax.rem(me_s + k, sp)
-        remote(buf.at[peer], buf.at[peer], send.at[k - 1], recv.at[peer], "sp", peer).wait_recv()
+    next_s, next_t = lax.rem(me_s + 1, sp), lax.rem(me_t + 1, tp)
 
     for k in range(1, sp):
-        to_sp(k, modsp, msp_send, msp_recv).start()
+        remote(
+            modsp.at[me_s], modsp.at[me_s], msp_send.at[0], msp_recv.at[0], "sp",
+            lax.rem(me_s + k, sp),
+        ).start()
+
+    def all_sp():
+        return whole(modsp.at[pl.ds(0, sp - 1)], msp_send, msp_recv, "sp", next_s)
+
+    def all_tp():
+        return whole(modtp.at[pl.ds(0, tp - 1)], mtp_send, mtp_recv, "tp", next_t)
 
     for copy in small[4:7]:
         copy.wait()
@@ -234,8 +242,7 @@
 
     lax.fori_loop(0, heads // 2, fill, 0)
 
-    for k in range(1, sp):
-        from_sp(k, modsp, msp_send, msp_recv)
+    all_sp().wait_recv()
     summed = modsp[0]
     for s in range(1, sp):
         summed = summed + modsp[s]
@@ -243,7 +250,7 @@
 
     def to_tp(k):
         return remote(
-            modtp.at[me_t], modtp.at[me_t], mtp_send.at[k - 1], mtp_recv.at[me_t], "tp",
+            modtp.at[me_t], modtp.at[me_t], mtp_send.at[0], mtp_recv.at[0], "tp",
             lax.rem(me_t + k, tp),
         )
 
@@ -252,8 +259,7 @@
     load_tokens.wait()
     for k in range(1, chips):
         across_part(k, early, chunk - early, tok.at[me_t]).start()
-    for c in range(chunks):
-        arrived(pair, c)
+    whole(tok.at[pair], pair_send, tok_recv, "tp", pair).wait_recv()
     for i in range(1, chunks):
         for k in range(1, chips):
             across(k, i).start()
@@ -261,35 +267,31 @@
     twin = me_s + 1 - 2 * (me_s % 2)
     steps = sp // 2
 
-    def context_copy(block, peer, index):
-        return remote(
-            ctxbuf.at[block], ctxbuf.at[block], ctx_send.at[index], ctx_recv.at[block], "sp", peer
+    def context_copy(block, peer):
+        return remote(
+            ctxbuf.at[block], ctxbuf.at[block], ctx_send.at[0], ctx_recv.at[block], "sp", peer
         )
 
     def fellow(m):
         return lax.rem(me_s + 2 * (m // 2 + 1 if m % 2 == 0 else steps - m // 2 - 1), sp)
 
     def context_arrived(block):
-        context_copy(block, twin, 0).wait_recv()
-
-    context_copy(me_s, twin, 0).start()
+        context_copy(block, twin).wait_recv()
+
+    context_copy(me_s, twin).start()
     for m in range(steps - 1):
-        context_copy(me_s, fellow(m), 1 + m).start()
+        context_copy(me_s, fellow(m)).start()
 
     def pass_context(begin, end):
         for m in range(begin, end):
             context_arrived(fellow(m))
-            context_copy(fellow(m), twin, steps + m).start()
+            context_copy(fellow(m), twin).start()
 
     lax.fori_loop(heads // 2, heads, fill, 0)
 
     load_o.start()
     load_q.wait()
-    for k in range(1, tp):
-        peer = lax.rem(me_t + k, tp)
-        remote(
-            modtp.at[peer], modtp.at[peer], mtp_send.at[k - 1], mtp_recv.at[peer], "tp", peer
-        ).wait_recv()
+    all_tp().wait_recv()
     piece = modtp.shape[2]
     for t in range(tp):
         mods[:, t * piece : (t + 1) * piece] = modtp[t]
@@ -463,8 +465,8 @@
         src = pl.ds(pl.multiple_of(p * piece, piece), piece)
         dst = pl.ds(pl.multiple_of(local * piece, piece), piece)
         return remote(
-            att.at[src, :], full.at[me_t, dst, :], att_send.at[p],
-            att_recv.at[me_t * per_dest + local], "tp", dest,
+            att.at[src, :], full.at[me_t, dst, :], att_send.at[0],
+            att_recv.at[jnp.where(dest // 2 == chip, 0, 1 + local)], "tp", dest,
         )
 
     def choose(index, for_upper, for_lower):
@@ -509,7 +511,7 @@
         swap, c = plan(i, core)
         block = far_chip * 2 + (core + swap) % 2
         arrived(block, c)
-        onward(k, i, block, c).start()
+        onward(block, c).start()
         if on_arrival is not None:
             on_arrival()
         project(block, c)
@@ -610,25 +612,22 @@
 
     tile = HEAD_DIM * divisor(d // HEAD_DIM, 4)
 
-    def await_piece(peer, j):
-        at = pl.ds(pl.multiple_of(j * piece, piece), piece)
-        remote(
-            full.at[peer, at, :], full.at[peer, at, :], att_send.at[0],
-            att_recv.at[peer * per_dest + j], "tp", peer,
-        ).wait_recv()
-
     def project_out(peer, at, lanes):
         return dot32(full[peer, at, :], wo[pl.ds(pl.multiple_of(peer * width, width), width), lanes])
 
-    for j in range(per_dest):
-        await_piece(pair, j)
-
-    def near_column(n, carry):
+    def own_column(n, carry):
         lanes = pl.ds(pl.multiple_of(n * tile, tile), tile)
-        partial[:, lanes] = project_out(me_t, slice(None), lanes) + project_out(pair, slice(None), lanes)
+        partial[:, lanes] = project_out(me_t, slice(None), lanes)
         return carry
 
-    lax.fori_loop(0, d // tile, near_column, 0, unroll=True)
+    def pair_column(n, carry):
+        lanes = pl.ds(pl.multiple_of(n * tile, tile), tile)
+        partial[:, lanes] += project_out(pair, slice(None), lanes)
+        return carry
+
+    lax.fori_loop(0, d // tile, own_column, 0, unroll=True)
+    whole(full.at[pair], att_send, att_recv, "tp", pair).wait_recv()
+    lax.fori_loop(0, d // tile, pair_column, 0, unroll=True)
 
     def far_piece(step, carry):
         j = per_dest - 1 - step
@@ -636,8 +635,8 @@
         peers = [
             lax.rem(chip + k, chips) * 2 + side for k in range(1, chips) for side in range(2)
         ]
-        for peer in peers:
-            await_piece(peer, j)
+        landed = full.at[pl.ds(0, tp - 2), at, :]
+        remote(landed, landed, att_send.at[0], att_recv.at[1 + j], "tp", pair).wait_recv()
 
         def column(n, inner):
             lanes = pl.ds(pl.multiple_of(n * tile, tile), tile)
@@ -653,28 +652,13 @@
 
     lax.fori_loop(0, per_dest, far_piece, 0)
 
-    for c in range(chunks):
-        beside(c).wait_send()
-        for k in range(1, chips):
-            across(k, c).wait_send()
-            onward(k, c, me_t, c).wait_send()
-    for k in range(1, sp):
-        to_sp(k, modsp, msp_send, msp_recv).wait_send()
-    context_copy(me_s, twin, 0).wait_send()
-    for m in range(steps - 1):
-        context_copy(me_s, twin, 1 + m).wait_send()
-        context_copy(me_s, twin, steps + m).wait_send()
-    for k in range(1, tp):
-        to_tp(k).wait_send()
-
-    def sent(p, carry):
-        @pl.when(p // per_dest != me_t)
-        def _():
-            hand(p).wait_send()
-
-        return carry
-
-    lax.fori_loop(0, rows // piece_rows, sent, 0)
+    whole(tok.at[pl.ds(0, 1)], pair_send, tok_recv, "tp", pair).wait_send()
+    whole(tok.at[pl.ds(0, chips - 1)], tok_send, tok_recv, "tp", pair).wait_send()
+    whole(tok.at[pl.ds(0, chips - 1)], fwd_send, tok_recv, "tp", pair).wait_send()
+    whole(att.at[pl.ds(0, tokens - count), :], att_send, att_recv, "tp", pair).wait_send()
+    whole(ctxbuf.at[pl.ds(0, sp - 1)], ctx_send, ctx_recv, "sp", next_s).wait_send()
+    all_sp().wait_send()
+    all_tp().wait_send()
 
     @pl.when(me_s > 0)
     def _():
@@ -719,7 +703,6 @@
     vmem = pl.BlockSpec(memory_space=pltpu.VMEM)
     hbm = pl.BlockSpec(memory_space=pltpu.HBM)
     sems = pltpu.SemaphoreType.DMA
-    hops = max(1, (chips - 1) * chunks)
     return pl.pallas_call(
         functools.partial(layer_kernel, sp, tp, chunks),
         in_specs=[hbm] * 15,
@@ -757,20 +740,20 @@
             pltpu.VMEM((2, 3 * span + ctx_count, span), bf),
             pltpu.VMEM((count, d), f32),
             sems((15,)),
-            sems((hops,)),
-            sems((chunks,)),
-            sems((hops,)),
-            sems((tp * chunks,)),
-            sems((sp,)),
-            sems((sp,)),
-            sems((tp,)),
-            sems((tp,)),
-            sems((sp,)),
+            sems((1,)),
+            sems((1,)),
+            sems((1,)),
+            sems((1 + (tp - 2) * chunks,)),
+            sems((1,)),
+            sems((1,)),
+            sems((1,)),
+            sems((1,)),
+            sems((1,)),
             sems((sp,)),
             sems((2,)),
             sems((2,)),
-            sems((tp * pieces,)),
-            sems((tp * pieces,)),
+            sems((1,)),
+            sems((1 + pieces,)),
         ],
         compiler_params=pltpu.CompilerParams(
             collective_id=0, has_side_effects=True, vmem_limit_bytes=VMEM_BYTES

time: 64 us -> 63.3 us (0.989)
  Pallas kernels: 62.7 us -> 62 us
    pallas_call x1, Pallas kernels: 62.7 us -> 62 us  [shards(): pl.pallas_call(functools.partial(layer_kernel, sp, tp, chunks), in_specs=...]
where the time goes in v5:
time: 63.3 us; the launch traced here: 63.1 us
  Pallas kernels  62 us (98%)
  local copies, waits for them, and re-layouts  1.15 us (2%)
    pallas_call x1, Pallas kernels, shards(): pl.pallas_call(functools.partial(layer_kernel, sp, tp, chunks), in_specs=...  62 us

profile of v5, /device:TPU:0, one launch (start us, length us, event | category | flops | bytes accessed | tf_op | source)
XLA Modules:
  0.0 63.1 jit_solution(4298722413936253850)
XLA Ops:
  0.0 62.0 %layer.1 = bf16[384,2048]{1,0:T(8,128)(2,1)S(1)} custom-call(f32[1,4]{1,0:T(1,128)} %bitcast.8, bf16[384,2048]{1,0:T(8,128)(2,1)} %resid.1, bf16[2,128]{1,0:T(2,128)(2,1)} %bitcast.9, bf16[256,512]{1,0:T(8,128)(2,1)} %mshift_hbm.1, bf16[256,512]{1,0:T(8,128)(2,1)} %mscale_hbm.1, bf16[256,512]{1,0:T(8,128)(2,1)} %mgate_hbm.1, f32[1,2048]{1,0:T(1,128)} %bitcast.7, ...), custom_call_target="tpu_custom_call" | custom-call | tf_op jit(solution)/shard_map/layer/pallas_call | solution.py:706
  62.0 1.1 %copy.17 = bf16[384,2048]{1,0:T(8,128)(2,1)} copy(bf16[384,2048]{1,0:T(8,128)(2,1)S(1)} %layer.1) | data formatting | bytes 3145728

commit v6 on v5

--- a/solution.py
+++ b/solution.py
@@ -80,7 +80,7 @@
     tok, wq, wk, wv, wo, qbuf, kvbuf, ctxbuf, ob_ref, table, modsp, modtp, mods, att, full,
     vt, ctxvt, score, prob, partial,
     load_sem, tok_send, pair_send, fwd_send, tok_recv, msp_send, msp_recv, mtp_send, mtp_recv,
-    ctx_send, ctx_recv, halo_send, halo_recv, att_send, att_recv,
+    ctx_send, ctx_recv, halo_send, halo_recv, att_send, att_recv, ready, go,
 ):
     me_s, me_t = lax.axis_index("sp"), lax.axis_index("tp")
     count, d = resid.shape
@@ -102,16 +102,18 @@
         )
 
     barrier = pltpu.get_barrier_semaphore()
-    for k in range(1, sp):
+
+    def signal(semaphore, axis, peer):
         pl.semaphore_signal(
-            barrier, inc=1, device_id={"sp": lax.rem(me_s + k, sp)},
-            device_id_type=pl.DeviceIdType.MESH,
-        )
+            semaphore, inc=1, device_id={axis: peer}, device_id_type=pl.DeviceIdType.MESH
+        )
+
     for k in range(1, tp):
-        pl.semaphore_signal(
-            barrier, inc=1, device_id={"tp": lax.rem(me_t + k, tp)},
-            device_id_type=pl.DeviceIdType.MESH,
-        )
+        other = lax.rem(me_t + k, tp)
+
+        @pl.when(other != 0)
+        def _():
+            signal(barrier, "tp", other)
 
     def load(index, src, dst):
         return pltpu.make_async_copy(src, dst, load_sem.at[index])
@@ -132,7 +134,18 @@
     load_tokens = load(base + 4, resid, tok.at[me_t])
     for copy in small[:6] + [load_tokens, load_k, load_v] + small[6:] + [load_q]:
         copy.start()
-    pl.semaphore_wait(barrier, sp + tp - 2)
+
+    @pl.when(me_t != 0)
+    def _():
+        pl.semaphore_wait(barrier, tp - 1)
+        signal(ready, "tp", 0)
+
+    @pl.when(me_t == 0)
+    def _():
+        pl.semaphore_wait(ready, tp - 1)
+        for k in range(1, sp):
+            signal(barrier, "sp", lax.rem(me_s + k, sp))
+
 
     def part(block, c):
         return tok.at[block, pl.ds(pl.multiple_of(c * chunk, chunk), chunk), :]
@@ -189,7 +202,7 @@
             "tp", pair,
         ).wait_recv()
 
-    early = chunk * 3 // 128 * 16 if chunk >= 128 else chunk // 2
+    early = chunk // 64 * 48 if chunk >= 128 else chunk // 2
     for k in range(1, chips):
         across_part(k, 0, early, resid).start()
     for c in range(chunks):
@@ -210,12 +223,6 @@
 
     next_s, next_t = lax.rem(me_s + 1, sp), lax.rem(me_t + 1, tp)
 
-    for k in range(1, sp):
-        remote(
-            modsp.at[me_s], modsp.at[me_s], msp_send.at[0], msp_recv.at[0], "sp",
-            lax.rem(me_s + k, sp),
-        ).start()
-
     def all_sp():
         return whole(modsp.at[pl.ds(0, sp - 1)], msp_send, msp_recv, "sp", next_s)
 
@@ -230,6 +237,22 @@
     own = ctxbuf.at[me_s]
     store_heads(own, 0, dot32(normed, wk[...]), kg[...])
     own[:, width:] = dot32(normed, wv[...]).astype(jnp.bfloat16)
+
+    @pl.when(me_t == 0)
+    def _():
+        pl.semaphore_wait(barrier, sp - 1)
+        for k in range(1, tp):
+            signal(go, "tp", k)
+
+    @pl.when(me_t != 0)
+    def _():
+        pl.semaphore_wait(go, 1)
+
+    for k in range(1, sp):
+        remote(
+            modsp.at[me_s], modsp.at[me_s], msp_send.at[0], msp_recv.at[0], "sp",
+            lax.rem(me_s + k, sp),
+        ).start()
 
     for copy in small[7:]:
         copy.wait()
@@ -546,6 +569,7 @@
             @pl.when(b == blocks - 1)
             def _():
                 wait_bottom()
+                send_down(upper)
                 prepare(blocks + 1)
 
             attend_block(b)
@@ -565,7 +589,7 @@
                     hand_block(early_block)
 
             far(1, i, hand_early)
-            send_down((lower & (i == 0)) | (upper & (i == 1)))
+            send_down(lower & (i == 0))
             send_up(lower & (i == 2))
 
             @pl.when(i == 1)
@@ -754,6 +778,8 @@
             sems((2,)),
             sems((1,)),
             sems((1 + pieces,)),
+            pltpu.SemaphoreType.REGULAR,
+            pltpu.SemaphoreType.REGULAR,
         ],
         compiler_params=pltpu.CompilerParams(
             collective_id=0, has_side_effects=True, vmem_limit_bytes=VMEM_BYTES

time: 63.3 us -> 62.7 us (level)
  the two profiles are of different devices: /device:TPU:0 before, /device:TPU:6 now
where the time goes in v6:
time: 62.7 us; the launch traced here: 62.5 us
  Pallas kernels  61.4 us (98%)
  local copies, waits for them, and re-layouts  1.15 us (2%)
    pallas_call x1, Pallas kernels, shards(): pl.pallas_call(functools.partial(layer_kernel, sp, tp, chunks), in_specs=...  61.4 us

profile of v6, /device:TPU:6, one launch (start us, length us, event | category | flops | bytes accessed | tf_op | source)
XLA Modules:
  0.0 62.5 jit_solution(18291930297589480465)
XLA Ops:
  0.0 61.4 %layer.1 = bf16[384,2048]{1,0:T(8,128)(2,1)S(1)} custom-call(f32[1,4]{1,0:T(1,128)} %bitcast.8, bf16[384,2048]{1,0:T(8,128)(2,1)} %resid.1, bf16[2,128]{1,0:T(2,128)(2,1)} %bitcast.9, bf16[256,512]{1,0:T(8,128)(2,1)} %mshift_hbm.1, bf16[256,512]{1,0:T(8,128)(2,1)} %mscale_hbm.1, bf16[256,512]{1,0:T(8,128)(2,1)} %mgate_hbm.1, f32[1,2048]{1,0:T(1,128)} %bitcast.7, ...), custom_call_target="tpu_custom_call" | custom-call | tf_op jit(solution)/shard_map/layer/pallas_call | solution.py:730
  61.4 1.1 %copy.17 = bf16[384,2048]{1,0:T(8,128)(2,1)} copy(bf16[384,2048]{1,0:T(8,128)(2,1)S(1)} %layer.1) | data formatting | bytes 3145728
